TPU v7x, 512 devices: a whole 4x4x16 slice. The times are simulated.
512 devices in a mesh: sp: 64 (over z, y), tp: 8 (over x, core).
Axes of the slice: x: 4, y: 4, z: 16, core: 2. Of those that a mesh axis runs over, the one named last changes fastest.
Arguments:
- query_logits: bfloat16 [8192, 1024], P('sp', 'tp'), may hold values from -6 to 6
- value_rows: bfloat16 [8192, 1024], P('sp', 'tp'), may hold values from -6 to 6
- onward_forget_logits: bfloat16 [8192, 1024], P('sp', 'tp'), may hold values from -5.5 to 5.5
- reverse_forget_logits: bfloat16 [8192, 1024], P('sp', 'tp'), may hold values from -5.5 to 5.5
- output_gate_logits: bfloat16 [8192, 1024], P('sp', 'tp'), may hold values from -6 to 6
- onward_floor_gap: float32 [1024], P('tp'), may hold values from 0 to 0.12, as said below
- reverse_floor_gap: float32 [1024], P('tp'), may hold values from 0 to 0.12, as said below
- extra_log_decay: float32 [8192, 8], P('sp', 'tp'), may hold values from -2.1 to 0
- per_head_gain: float32 [128], replicated, may hold values from 0.1 to 1.9
- residual: bfloat16 [8192, 2048], P('sp', 'tp'), may hold values from -8 to 8
- output_matrix: bfloat16 [1024, 2048], P(None, 'tp'), may hold values from -0.375 to 0.375
- inner_norm_gain: float32 [2048], P('tp'), may hold values from 0.1 to 1.9
- inner_norm_bias: float32 [2048], P('tp'), may hold values from -1.5 to 1.5
- gate_matrix: bfloat16 [2048, 5632], P('sp', 'tp'), may hold values from -0.125 to 0.125
- up_matrix: bfloat16 [2048, 5632], P('sp', 'tp'), may hold values from -0.125 to 0.125
- down_matrix: bfloat16 [5632, 2048], P('tp', 'sp'), may hold values from -0.15625 to 0.15625
- closing_norm_gain: float32 [2048], P('tp'), may hold values from 0.1 to 1.9
- closing_norm_bias: float32 [2048], P('tp'), may hold values from -1.5 to 1.5
Outputs:
- layer_output: bfloat16 [8192, 2048], P('sp', 'tp')
Inputs may be any that keep to these rules, and one draw needn't show every extreme that they name: `onward_floor_gap`: positive. `reverse_floor_gap`: positive.
All inputs are finite; a program needn't handle non-finite values.
Results may differ from a plain program's by a relative error of at most 0.014.
Values may be sent and summed in bfloat16 or wider, within the bound.
No kernel may reach another device: no remote copies, remote signals or barrier semaphores. Data moves between devices by JAX's collectives and lax.ppermute only.
A program may use at most 64 MiB of HBM per device.

v0:
```python
import jax
import jax.numpy as jnp
from jax import lax
from jax.experimental import pallas as pl
from jax.experimental.pallas import tpu as pltpu
from jax.sharding import Mesh
from jax.sharding import PartitionSpec as P


D = 2048
Z = ("zb", "zr")
NEAR = ("zr", "ya", "yb")
SP = ("zb", "zr", "ya", "yb")
TP = ("x", "c")
HALF = 352
SLICE = 16
BLOCK = 8

highest_precision = lax.Precision.HIGHEST
alpha_mix = 2.0**0.25
norm_eps = 1e-05
head_eps = 1e-06


def exact_dot(a, b, dims=((1,), (0,))):
    return lax.dot_general(
        a, b, (dims, ((), ())), precision=highest_precision, preferred_element_type=jnp.float32
    )


def two_terms(x):
    high = x.astype(jnp.bfloat16).astype(jnp.float32)
    return high, (x - high).astype(jnp.bfloat16).astype(jnp.float32)


def local_kernel(
    query_ref,
    value_ref,
    onward_ref,
    reverse_ref,
    onward_gap_ref,
    reverse_gap_ref,
    extra_ref,
    inner_ref,
    queries_ref,
    packed_ref,
    rows_ref,
):
    rows, width = query_ref.shape
    logits = query_ref[...].astype(jnp.float32)
    query = logits / (1.0 + jnp.exp(-logits))
    values = value_ref[...].astype(jnp.float32)
    extra = extra_ref[...]
    at = lax.broadcasted_iota(jnp.int32, (rows, rows), 0)
    source = lax.broadcasted_iota(jnp.int32, (rows, rows), 1)
    ones = jnp.ones((rows, width), jnp.float32)
    inner = jnp.zeros_like(query)
    rows_ref[:, 2 * SLICE :, :] = jnp.zeros((BLOCK, 8, width), jnp.float32)
    for side, (forget_ref, gap_ref, seen, last) in enumerate(
        (
            (onward_ref, onward_gap_ref, at >= source, rows - 1),
            (reverse_ref, reverse_gap_ref, at <= source, 0),
        )
    ):
        seen = seen.astype(jnp.float32)
        keys = gap_ref[...] / (1.0 + jnp.exp(forget_ref[...].astype(jnp.float32)))
        running = exact_dot(seen, jnp.log1p(-keys)) + exact_dot(seen * extra, ones)
        total = running[last : last + 1]
        decayed_query = query * jnp.exp(running)
        scores = exact_dot(decayed_query, keys * jnp.exp(-running), ((1,), (1,))) * seen
        inner = inner + exact_dot(scores, values)
        queries_ref[:, width * side : width * (side + 1)] = decayed_query
        state = exact_dot(values, keys * jnp.exp(total - running), ((0,), (0,)))
        terms = two_terms(total)
        for y in range(BLOCK):
            rows_ref[y, SLICE * side : SLICE * (side + 1), :] = state[
                SLICE * y : SLICE * (y + 1)
            ]
            for t in range(2):
                at_row = 2 * SLICE + 2 * side + t
                rows_ref[y, at_row : at_row + 1, :] = terms[t]
    packed_ref[...] = rows_ref[...].astype(jnp.bfloat16)
    inner_ref[...] = inner


def near(*arrays):
    return [pltpu.with_memory_space_constraint(a, pltpu.VMEM) for a in arrays]


def local_pass(*arrays):
    rows, width = arrays[0].shape
    return pl.pallas_call(
        local_kernel,
        out_shape=[
            pltpu.VMEM((rows, width), jnp.float32),
            pltpu.VMEM((rows, 2 * width), jnp.float32),
            pltpu.VMEM((BLOCK, 2 * SLICE + 8, width), jnp.bfloat16),
        ],
        scratch_shapes=[pltpu.VMEM((BLOCK, 2 * SLICE + 8, width), jnp.float32)],
        compiler_params=pltpu.CompilerParams(vmem_limit_bytes=6 << 20),
        name="local",
    )(*near(*arrays))


def plane_parts(arrived_ref):
    parts = []
    for side in range(2):
        part = []
        for y in range(BLOCK):
            block = arrived_ref[y].astype(jnp.float32)
            decay = block[2 * SLICE + 2 * side : 2 * SLICE + 2 * side + 1]
            decay = decay + block[2 * SLICE + 2 * side + 1 : 2 * SLICE + 2 * side + 2]
            part.append((decay, block[SLICE * side : SLICE * (side + 1)]))
        parts.append(part)
    return parts


def plane_kernel(z_ref, arrived_ref, out_ref, rows_ref):
    forward, backward = plane_parts(arrived_ref)
    wholes = []
    for part in (forward, backward[::-1]):
        decay, state = part[0]
        for next_decay, next_state in part[1:]:
            decay, state = decay + next_decay, jnp.exp(next_decay) * state + next_state
        wholes.append((decay, state))
    for side, (decay, state) in enumerate(wholes):
        rows_ref[side] = jnp.zeros(rows_ref.shape[1:], jnp.float32)
        rows_ref[side, :SLICE, :] = state
        for t, term in enumerate(two_terms(decay)):
            rows_ref[side, SLICE + t : SLICE + t + 1, :] = term
    ahead, behind = rows_ref[0].astype(jnp.bfloat16), rows_ref[1].astype(jnp.bfloat16)
    z = z_ref[0]
    for other in range(out_ref.shape[0]):

        @pl.when(other > z)
        def _():
            out_ref[other] = ahead

        @pl.when(other <= z)
        def _():
            out_ref[other] = behind


def before_kernel(z_ref, planes_ref, arrived_ref, out_ref):
    z = z_ref[0]
    planes = planes_ref.shape[0]
    width = planes_ref.shape[2]
    states = []
    for order in (range(planes), reversed(range(planes))):
        state = jnp.zeros((SLICE, width), jnp.float32)
        for other in order:
            block = planes_ref[other].astype(jnp.float32)
            decay = block[SLICE : SLICE + 1] + block[SLICE + 1 : SLICE + 2]
            passed = other < z if not states else other > z
            state = jnp.where(passed, jnp.exp(decay) * state + block[:SLICE], state)
        states.append(state)
    forward, backward = plane_parts(arrived_ref)
    for side, part in enumerate((forward, backward)):
        state = states[side]
        for y in range(BLOCK) if side == 0 else reversed(range(BLOCK)):
            out_ref[y, SLICE * side : SLICE * (side + 1)] = state.astype(jnp.bfloat16)
            decay, own = part[y]
            state = jnp.exp(decay) * state + own


def states_around(packed):
    z = lax.axis_index("zb").astype(jnp.int32)[None]
    planes = lax.axis_size("zb")
    width = packed.shape[2]
    (arrived,) = near(lax.all_to_all(packed, NEAR, 0, 0, tiled=True))
    totals = pl.pallas_call(
        plane_kernel,
        in_specs=[SMEM, VMEM],
        out_specs=VMEM,
        out_shape=pltpu.VMEM((planes, SLICE + 8, width), jnp.bfloat16),
        scratch_shapes=[pltpu.VMEM((2, SLICE + 8, width), jnp.float32)],
        compiler_params=pltpu.CompilerParams(vmem_limit_bytes=4 << 20),
        name="plane",
    )(z, arrived)
    (others,) = near(lax.all_to_all(totals, "zb", 0, 0, tiled=True))
    before = pl.pallas_call(
        before_kernel,
        in_specs=[SMEM, VMEM, VMEM],
        out_specs=VMEM,
        out_shape=pltpu.VMEM((BLOCK, 2 * SLICE, width), jnp.bfloat16),
        compiler_params=pltpu.CompilerParams(vmem_limit_bytes=4 << 20),
        name="before",
    )(z, others, arrived)
    return lax.all_to_all(before, NEAR, 0, 0, tiled=True)


def gated_kernel(back_ref, inner_ref, queries_ref, gain_ref, gate_ref, out_ref):
    width = inner_ref.shape[1]
    mixed = inner_ref[...]
    for side in range(2):
        state = [back_ref[y, SLICE * side : SLICE * (side + 1)] for y in range(BLOCK)]
        state = jnp.concatenate([part.astype(jnp.float32) for part in state], axis=0)
        queries = queries_ref[:, width * side : width * (side + 1)]
        mixed = mixed + exact_dot(queries, state, ((1,), (1,)))
    mean = jnp.mean(mixed * mixed, axis=1, keepdims=True)
    normed = mixed * lax.rsqrt(mean + head_eps) * gain_ref[...]
    gate = gate_ref[...].astype(jnp.float32)
    gated = (normed * (gate / (1.0 + jnp.exp(-gate)))).astype(jnp.bfloat16)
    for peer in range(out_ref.shape[0]):
        out_ref[peer] = gated


def gated_rows(*arrays):
    return pl.pallas_call(
        gated_kernel,
        out_shape=pltpu.VMEM((8, *arrays[1].shape), jnp.bfloat16),
        compiler_params=pltpu.CompilerParams(vmem_limit_bytes=4 << 20),
        name="gated",
    )(*near(*arrays))


SMEM = pl.BlockSpec(memory_space=pltpu.SMEM)
VMEM = pl.BlockSpec(memory_space=pltpu.VMEM)
ANY = pl.BlockSpec(memory_space=pl.ANY)


def turn_kernel(in_ref, out_ref):
    for kind in range(3):
        rows = jnp.concatenate([in_ref[y, kind] for y in range(4)], axis=0)
        out_ref[kind] = rows.T


def gathered_weights(gate, up, down):
    both = jnp.stack([gate, up, down.T])
    halves = [both[:, :, :HALF], both[:, :, HALF:]]
    arrived = lax.all_to_all(jnp.stack(halves + halves), ("ya", "yb"), 0, 0, tiled=True)
    shard = pl.pallas_call(
        turn_kernel,
        out_shape=jax.ShapeDtypeStruct((3, HALF, 128), jnp.bfloat16),
        compiler_params=pltpu.CompilerParams(vmem_limit_bytes=6 << 20),
        name="turn",
    )(*near(arrived)).reshape(3 * HALF, 128)
    weights = lax.all_gather(shard, Z, axis=0, tiled=True).reshape(-1, 3, HALF, 128)
    return pltpu.with_memory_space_constraint(weights, pltpu.HBM)


def exact_terms(x):
    terms = []
    for _ in range(3):
        term = lax.reduce_precision(x, 8, 7)
        terms.append(term.astype(jnp.bfloat16))
        x = x - term
    return terms


SWAP = ((0, 1), (1, 0))


def spread_over_x(output_matrix, residual, gain, bias):
    other = lax.ppermute(residual, "yb", SWAP)
    first = lax.axis_index("yb") == 0
    vectors = jnp.stack(exact_terms(gain) + exact_terms(bias))
    block = jnp.concatenate(
        [
            output_matrix,
            jnp.where(first, residual, other),
            jnp.where(first, other, residual),
            jnp.pad(vectors, ((0, 10), (0, 0))),
        ]
    )
    count = lax.axis_size("x")
    return [block] + [
        lax.ppermute(block, "x", [(i, (i + k) % count) for i in range(count)])
        for k in range(1, count)
    ]


def middle_kernel(place_ref, gated_ref, *refs):
    block_refs, (out_ref, own_ref, whole_ref, before_ref) = refs[:8], refs[8:]
    heads, rows = 8, gated_ref.shape[2]
    count = 2 * rows
    for core in range(2):
        for pair in range(2):
            for x in range(4):
                head = 2 * x + core
                whole_ref[pair * rows : (pair + 1) * rows, 128 * head : 128 * head + 128] = (
                    gated_ref[core, 4 * pair + x]
                )
    whole = whole_ref[...]
    inner = whole.shape[1]
    total = jnp.zeros((count, 1), jnp.float32)
    for b in range(heads):
        mixer = jnp.dot(whole, block_refs[b][:inner], preferred_element_type=jnp.float32)
        residual = block_refs[b][inner : inner + count].astype(jnp.float32)
        before = alpha_mix * residual + mixer
        before_ref[b] = before
        total = total + jnp.sum(before, axis=1, keepdims=True)
    mean = total / D
    spread = jnp.zeros((count, 1), jnp.float32)
    for b in range(heads):
        centre = before_ref[b] - mean
        spread = spread + jnp.sum(centre * centre, axis=1, keepdims=True)
    scale = lax.rsqrt(spread / D + norm_eps)
    for b in range(heads):
        vectors = block_refs[b][inner + count : inner + count + 16].astype(jnp.float32)
        gain = vectors[0:1] + vectors[1:2] + vectors[2:3]
        bias = vectors[3:4] + vectors[4:5] + vectors[5:6]
        normed = (before_ref[b] - mean) * scale * gain + bias
        normed = normed.astype(jnp.bfloat16)
        out_ref[place_ref[b]] = normed
        if b == 0:
            own_ref[...] = jnp.where(place_ref[heads] == 0, normed[:rows], normed[rows:])


def middle_rows(gated, blocks):
    rows, width = gated.shape[2], blocks[0].shape[1]
    x, core = lax.axis_index("x"), lax.axis_index("c")
    place = [2 * ((x - b // 2 + 4) % 4) + (core + b) % 2 for b in range(8)]
    place = jnp.stack(place + [lax.axis_index("yb")])
    vmem = pl.BlockSpec(memory_space=pltpu.VMEM)
    return pl.pallas_call(
        middle_kernel,
        in_specs=[pl.BlockSpec(memory_space=pltpu.SMEM)] + [vmem] * 9,
        out_specs=[vmem, vmem],
        out_shape=[
            pltpu.VMEM((8, 2 * rows, width), jnp.bfloat16),
            pltpu.VMEM((rows, width), jnp.bfloat16),
        ],
        scratch_shapes=[
            pltpu.VMEM((2 * rows, 8 * 128), jnp.bfloat16),
            pltpu.VMEM((8, 2 * rows, width), jnp.float32),
        ],
        compiler_params=pltpu.CompilerParams(vmem_limit_bytes=14 << 20),
        name="middle",
    )(place.astype(jnp.int32), *near(gated), *blocks)


def leaving(hidden, down_ref, block):
    wide = jnp.concatenate([down_ref[2 * block], down_ref[2 * block + 1]], axis=1)
    return jnp.dot(hidden, wide, preferred_element_type=jnp.float32)


def down_copies(core, weights_ref, leave_ref, sem_ref):
    copies = []
    for s in range(4):
        copies.append(
            pltpu.make_async_copy(
                weights_ref.at[pl.ds(4 * s + 2 * core, 2), 2],
                leave_ref.at[pl.ds(2 * s, 2)],
                sem_ref.at[s],
            )
        )
    return copies


def enter_kernel(
    core_ref, rows_ref, weights_ref, send_ref, hidden_ref, enter_ref, leave_ref, enter_sem, leave_sem
):
    parts, each = 4, 4
    copies = []
    for s in range(parts):
        copies.append(
            pltpu.make_async_copy(
                weights_ref.at[pl.ds(s * each, each), pl.ds(0, 2)],
                enter_ref.at[pl.ds(s * each, each)],
                enter_sem.at[s],
            )
        )
    downs = down_copies(1 - core_ref[0], weights_ref, leave_ref, leave_sem)
    for copy in copies + downs:
        copy.start()
    sums = [0.0, 0.0]
    for s in range(parts):
        x = jnp.concatenate([rows_ref[2 * s], rows_ref[2 * s + 1]], axis=1)
        copies[s].wait()
        for kind in range(2):
            wide = [enter_ref[each * s + j, kind] for j in range(each)]
            sums[kind] += lax.dot_general(
                x,
                jnp.concatenate(wide, axis=1),
                (((1,), (1,)), ((), ())),
                preferred_element_type=jnp.float32,
            )
    gate, up = sums
    hidden = (gate / (1.0 + jnp.exp(-gate)) * up).astype(jnp.bfloat16)
    hidden_ref[...] = hidden
    rows = send_ref.shape[2]
    for s in range(4):
        downs[s].wait()
        product = leaving(hidden, leave_ref, s).astype(jnp.bfloat16)
        send_ref[0, s] = product[:rows]
        send_ref[1, s] = product[rows:]


def leave_kernel(core_ref, hidden_ref, weights_ref, out_ref, leave_ref, leave_sem):
    downs = down_copies(core_ref[0], weights_ref, leave_ref, leave_sem)
    for copy in downs:
        copy.start()
    hidden = hidden_ref[...]
    rows = out_ref.shape[2]
    for s in range(4):
        downs[s].wait()
        product = leaving(hidden, leave_ref, s)
        out_ref[0, s] = product[:rows]
        out_ref[1, s] = product[rows:]


def join_kernel(mine_ref, other_ref, out_ref):
    for pair in range(2):
        for s in range(4):
            total = mine_ref[pair, s] + other_ref[pair, s].astype(jnp.float32)
            out_ref[2 * s + pair] = total.astype(jnp.bfloat16)


def feed_enter(core, rows, weights):
    blocks, count, width = rows.shape
    return pl.pallas_call(
        enter_kernel,
        in_specs=[SMEM, VMEM, ANY],
        out_specs=[VMEM, VMEM],
        out_shape=[
            pltpu.VMEM((2, blocks // 2, count // 2, width), jnp.bfloat16),
            pltpu.VMEM((count, HALF), jnp.bfloat16),
        ],
        scratch_shapes=[
            pltpu.VMEM((16, 2, HALF, 128), jnp.bfloat16),
            pltpu.VMEM((8, HALF, 128), jnp.bfloat16),
            pltpu.SemaphoreType.DMA((4,)),
            pltpu.SemaphoreType.DMA((4,)),
        ],
        cost_estimate=pl.CostEstimate(
            flops=5 * count * D * HALF, bytes_accessed=5 * D * HALF, transcendentals=count * HALF
        ),
        compiler_params=pltpu.CompilerParams(vmem_limit_bytes=16 << 20),
        name="feed_enter",
    )(core, *near(rows), weights)


def feed_leave(core, hidden, weights):
    count = hidden.shape[0]
    return pl.pallas_call(
        leave_kernel,
        in_specs=[SMEM, VMEM, ANY],
        out_specs=VMEM,
        out_shape=pltpu.VMEM((2, 4, count // 2, 256), jnp.float32),
        scratch_shapes=[
            pltpu.VMEM((8, HALF, 128), jnp.bfloat16),
            pltpu.SemaphoreType.DMA((4,)),
        ],
        cost_estimate=pl.CostEstimate(
            flops=count * D * HALF, bytes_accessed=D * HALF, transcendentals=0
        ),
        compiler_params=pltpu.CompilerParams(vmem_limit_bytes=8 << 20),
        name="feed_leave",
    )(core, *near(hidden), weights)


def joined(mine, other):
    return pl.pallas_call(
        join_kernel,
        out_shape=pltpu.VMEM((8, *mine.shape[2:]), jnp.bfloat16),
        compiler_params=pltpu.CompilerParams(vmem_limit_bytes=8 << 20),
        name="join",
    )(*near(mine, other))


def diagonal_of(rows):
    at = lax.broadcasted_iota(jnp.int32, (rows, rows), 0)
    return (at == lax.broadcasted_iota(jnp.int32, (rows, rows), 1)).astype(jnp.float32)


def total_kernel(arrived_ref, own_ref, before_ref, moments_ref):
    feed = arrived_ref[0].astype(jnp.float32)
    for peer in range(1, arrived_ref.shape[0]):
        feed = feed + arrived_ref[peer].astype(jnp.float32)
    before = alpha_mix * own_ref[...].astype(jnp.float32) + feed
    before_ref[...] = before
    diagonal = diagonal_of(before.shape[0])
    moments = []
    for value in (before, before * before):
        column = jnp.sum(value, axis=1, keepdims=True)
        moments.append(jnp.sum(diagonal * column, axis=0, keepdims=True))
    moments = jnp.concatenate(moments, axis=1)
    for peer in range(moments_ref.shape[0]):
        moments_ref[peer] = moments


def closing_kernel(moments_ref, before_ref, gain_ref, bias_ref, out_ref):
    moments = moments_ref[0]
    for peer in range(1, moments_ref.shape[0]):
        moments = moments + moments_ref[peer]
    rows = before_ref.shape[0]
    mean = moments[:, :rows] / D
    spread = moments[:, rows:] / D - mean * mean
    diagonal = diagonal_of(rows)
    column = jnp.sum(diagonal * mean, axis=1, keepdims=True)
    factor = jnp.sum(diagonal * lax.rsqrt(spread + norm_eps), axis=1, keepdims=True)
    out_ref[...] = ((before_ref[...] - column) * factor * gain_ref[...] + bias_ref[...]).astype(
        jnp.bfloat16
    )


def layer(
    query_logits,
    value_rows,
    onward_forget_logits,
    reverse_forget_logits,
    output_gate_logits,
    onward_floor_gap,
    reverse_floor_gap,
    extra_log_decay,
    per_head_gain,
    residual,
    output_matrix,
    inner_norm_gain,
    inner_norm_bias,
    gate_matrix,
    up_matrix,
    down_matrix,
    closing_norm_gain,
    closing_norm_bias,
):
    weights = gathered_weights(gate_matrix, up_matrix, down_matrix)
    rows = query_logits.shape[0]
    inner, queries, packed = local_pass(
        query_logits,
        value_rows,
        onward_forget_logits,
        reverse_forget_logits,
        onward_floor_gap[None],
        reverse_floor_gap[None],
        extra_log_decay.reshape(1, rows),
    )
    packed, output_matrix, residual = lax.optimization_barrier((packed, output_matrix, residual))
    back = states_around(packed)
    blocks = spread_over_x(output_matrix, residual, inner_norm_gain, inner_norm_bias)
    gated = gated_rows(back, inner, queries, per_head_gain[None], output_gate_logits)
    everyone = lax.all_to_all(gated, ("yb", "x"), 0, 0, tiled=True)
    everyone = lax.all_gather(everyone, "c")
    both = []
    for block in blocks:
        both += [block, lax.ppermute(block, "c", SWAP)]
    middle, own = middle_rows(everyone, both)
    core = lax.axis_index("c").astype(jnp.int32)[None]
    send, hidden = feed_enter(core, middle, weights)
    other = lax.ppermute(send, "c", SWAP)
    mine = feed_leave(core, hidden, weights)
    shares = lax.all_to_all(joined(mine, other), ("x", "yb"), 0, 0, tiled=True)
    before_final, moments = pl.pallas_call(
        total_kernel,
        out_shape=[
            pltpu.VMEM(own.shape, jnp.float32),
            pltpu.VMEM((8, 1, 2 * rows), jnp.float32),
        ],
        compiler_params=pltpu.CompilerParams(vmem_limit_bytes=4 << 20),
        name="total",
    )(*near(shares, own))
    moments = lax.all_to_all(moments, TP, 0, 0, tiled=True)
    return pl.pallas_call(
        closing_kernel,
        out_shape=jax.ShapeDtypeStruct(own.shape, jnp.bfloat16),
        compiler_params=pltpu.CompilerParams(vmem_limit_bytes=4 << 20),
        name="closing",
    )(*near(moments, before_final, closing_norm_gain[None], closing_norm_bias[None]))


def solution(mesh):
    torus = Mesh(mesh.devices.reshape(8, 2, 2, 2, 4, 2), ("zb", "zr", "ya", "yb", "x", "c"))
    in_specs = (
        P(SP, TP),
        P(SP, TP),
        P(SP, TP),
        P(SP, TP),
        P(SP, TP),
        P(TP),
        P(TP),
        P(SP, TP),
        P(),
        P(SP, TP),
        P(None, TP),
        P(TP),
        P(TP),
        P(SP, TP),
        P(SP, TP),
        P(TP, SP),
        P(TP),
        P(TP),
    )
    out_specs = P(SP, TP)
    return jax.shard_map(layer, mesh=torus, in_specs=in_specs, out_specs=out_specs, check_vma=False)
```

profile of v0, /device:TPU:1, one launch (start us, length us, event | category | flops | bytes accessed | tf_op | source)
XLA Modules:
  0.0 144.7 jit_solution(9074375141851537854)
XLA Ops:
  7.8 10.5 %all_to_all.35.in_ref = bf16[4,3,32,352]{3,2,1,0:T(8,128)(2,1)S(1)} all-to-all(bf16[4,3,32,352]{3,2,1,0:T(8,128)(2,1)S(1)} %pad_maximum_fusion), channel_id=1, replica_groups=mesh['zb'=8,'zr'=2,'ya'=2,'yb'=2,'x'=4,'c'=2] {'ya','yb'}, dimensions={0} | all-to-all | bytes 540672 | tf_op jit(solution)/shard_map/all_to_all | solution.py:231
  19.2 2.0 %local.1 = (f32[128,128]{1,0:T(8,128)S(1)}, f32[128,256]{1,0:T(8,128)S(1)}, bf16[8,40,128]{2,1,0:T(8,128)(2,1)}) custom-call(bf16[128,128]{1,0:T(8,128)(2,1)S(1)} %copy-done.3, bf16[128,128]{1,0:T(8,128)(2,1)S(1)} %copy-done.4, bf16[128,128]{1,0:T(8,128)(2,1)S(1)} %copy-done.5, bf16[128,128]{1,0:T(8,128)(2,1)S(1)} %copy-done.6, f32[1,128]{1,0:T(1,128)S(1)} %bitcast.32, ...), custom_call_target="tpu_custom_call" | custom-call | tf_op jit(solution)/shard_map/local/pallas_call | solution.py:92
  21.2 2.2 %collective-permute-start = (bf16[128,256]{1,0:T(8,128)(2,1)S(1)}, bf16[128,256]{1,0:T(8,128)(2,1)S(1)}, u32[]{:S(2)}, u32[]{:S(2)}) collective-permute-start(bf16[128,256]{1,0:T(8,128)(2,1)S(1)} %copy-done.14), channel_id=1, source_target_pairs={{0,8},{8,0},{1,9},{9,1},{2,10},{10,2},{3,11},{11,3},{4,12},{12,4},... | collective-permute-start | bytes 196616 | tf_op jit(solution)/shard_map/ppermute | solution.py:255
  23.5 2.7 %collective-permute-done = bf16[128,256]{1,0:T(8,128)(2,1)S(1)} collective-permute-done((bf16[128,256]{1,0:T(8,128)(2,1)S(1)}, bf16[128,256]{1,0:T(8,128)(2,1)S(1)}, u32[]{:S(2)}, u32[]{:S(2)}) %collective-permute-start) | collective-permute-done | bytes 65568 | tf_op jit(solution)/shard_map/ppermute | solution.py:255
  26.3 3.3 %collective-permute-start.2 = (bf16[1296,256]{1,0:T(8,128)(2,1)S(1)}, bf16[1296,256]{1,0:T(8,128)(2,1)S(1)}, u32[]{:S(2)}, u32[]{:S(2)}) collective-permute-start(bf16[1296,256]{1,0:T(8,128)(2,1)S(1)} %fusion.1.refs_0_), channel_id=1, source_target_pairs={{0,2},{2,4},{4,6},{6,0},{1,3},{3,5},{5,7},{7,1},{8,10},{10,12},{12... | collective-permute-start | bytes 1990664 | tf_op jit(solution)/shard_map/ppermute | solution.py:268
  29.6 4.4 %collective-permute-start.4 = (bf16[1296,256]{1,0:T(8,128)(2,1)S(1)}, bf16[1296,256]{1,0:T(8,128)(2,1)S(1)}, u32[]{:S(2)}, u32[]{:S(2)}) collective-permute-start(bf16[1296,256]{1,0:T(8,128)(2,1)S(1)} %fusion.1.refs_0_), channel_id=1, source_target_pairs={{0,4},{2,6},{4,0},{6,2},{1,5},{3,7},{5,1},{7,3},{8,12},{10,14},{12... | collective-permute-start | bytes 1990664 | tf_op jit(solution)/shard_map/ppermute | solution.py:268
  33.9 3.1 %collective-permute-start.6 = (bf16[1296,256]{1,0:T(8,128)(2,1)S(1)}, bf16[1296,256]{1,0:T(8,128)(2,1)S(1)}, u32[]{:S(2)}, u32[]{:S(2)}) collective-permute-start(bf16[1296,256]{1,0:T(8,128)(2,1)S(1)} %fusion.1.refs_0_), channel_id=1, source_target_pairs={{0,6},{2,0},{4,2},{6,4},{1,7},{3,1},{5,3},{7,5},{8,14},{10,8},{12,... | collective-permute-start | bytes 1990664 | tf_op jit(solution)/shard_map/ppermute | solution.py:268
  37.0 3.7 %all-to-all-start = ((bf16[8,40,128]{2,1,0:T(8,128)(2,1)}), bf16[8,40,128]{2,1,0:T(8,128)(2,1)S(1)}, u32[]{:S(2)}, u32[]{:S(2)}) async-start(bf16[8,40,128]{2,1,0:T(8,128)(2,1)} %get-tuple-element.18), calls=%async_computation | async-start | bytes 163840 | tf_op jit(solution)/shard_map/all_to_all | solution.py:170
  40.7 5.8 %all-to-all-done.arrived_ref = bf16[8,40,128]{2,1,0:T(8,128)(2,1)S(1)} async-done(((bf16[8,40,128]{2,1,0:T(8,128)(2,1)}), bf16[8,40,128]{2,1,0:T(8,128)(2,1)S(1)}, u32[]{:S(2)}, u32[]{:S(2)}) %all-to-all-start) | async-done | bytes 81952 | tf_op jit(solution)/shard_map/all_to_all | solution.py:170
  47.2 14.3 %all-to-all-start.1 = ((bf16[8,24,128]{2,1,0:T(8,128)(2,1)}), bf16[8,24,128]{2,1,0:T(8,128)(2,1)S(1)}, u32[]{:S(2)}, u32[]{:S(2)}) async-start(bf16[8,24,128]{2,1,0:T(8,128)(2,1)} %plane.1), calls=%async_computation.1 | async-start | bytes 98304 | tf_op jit(solution)/shard_map/all_to_all | solution.py:180
  61.5 7.3 %collective-permute-start.1 = (bf16[1296,256]{1,0:T(8,128)(2,1)S(1)}, bf16[1296,256]{1,0:T(8,128)(2,1)}, u32[]{:S(2)}, u32[]{:S(2)}) collective-permute-start(bf16[1296,256]{1,0:T(8,128)(2,1)S(1)} %fusion.1.refs_0_), channel_id=1, source_target_pairs={{0,1},{1,0},{2,3},{3,2},{4,5},{5,4},{6,7},{7,6},{8,9},{9,8},{10,11... | collective-permute-start | bytes 1990664 | tf_op jit(solution)/shard_map/ppermute | solution.py:537
  68.8 1.9 %collective-permute-start.3 = (bf16[1296,256]{1,0:T(8,128)(2,1)S(1)}, bf16[1296,256]{1,0:T(8,128)(2,1)}, u32[]{:S(2)}, u32[]{:S(2)}) collective-permute-start(bf16[1296,256]{1,0:T(8,128)(2,1)S(1)} %collective-permute-done.2.refs_2_), channel_id=1, source_target_pairs={{0,1},{1,0},{2,3},{3,2},{4,5},{5,4},{6,7},{7,6},{8,9},{9,8},{10,11... | collective-permute-start | bytes 1990664 | tf_op jit(solution)/shard_map/ppermute | solution.py:537
  70.7 2.4 %collective-permute-start.5 = (bf16[1296,256]{1,0:T(8,128)(2,1)S(1)}, bf16[1296,256]{1,0:T(8,128)(2,1)}, u32[]{:S(2)}, u32[]{:S(2)}) collective-permute-start(bf16[1296,256]{1,0:T(8,128)(2,1)S(1)} %collective-permute-done.4.refs_4_), channel_id=1, source_target_pairs={{0,1},{1,0},{2,3},{3,2},{4,5},{5,4},{6,7},{7,6},{8,9},{9,8},{10,11... | collective-permute-start | bytes 1990664 | tf_op jit(solution)/shard_map/ppermute | solution.py:537
  73.2 1.9 %collective-permute-start.7 = (bf16[1296,256]{1,0:T(8,128)(2,1)S(1)}, bf16[1296,256]{1,0:T(8,128)(2,1)}, u32[]{:S(2)}, u32[]{:S(2)}) collective-permute-start(bf16[1296,256]{1,0:T(8,128)(2,1)S(1)} %collective-permute-done.6.refs_6_), channel_id=1, source_target_pairs={{0,1},{1,0},{2,3},{3,2},{4,5},{5,4},{6,7},{7,6},{8,9},{9,8},{10,11... | collective-permute-start | bytes 1990664 | tf_op jit(solution)/shard_map/ppermute | solution.py:537
  75.2 8.0 %all_to_all.36.back_ref = bf16[8,32,128]{2,1,0:T(8,128)(2,1)S(1)} all-to-all(bf16[8,32,128]{2,1,0:T(8,128)(2,1)S(1)} %before.1), channel_id=1, replica_groups=mesh['zb'=8,'zr'=2,'ya'=2,'yb'=2,'x'=4,'c'=2] {'zr','ya','yb'}, dimensions={0} | all-to-all | bytes 131072 | tf_op jit(solution)/shard_map/all_to_all | solution.py:189
  84.3 3.4 %all-to-all-start.3 = ((bf16[8,128,128]{2,1,0:T(8,128)(2,1)}), bf16[8,128,128]{2,1,0:T(8,128)(2,1)S(1)}, u32[]{:S(2)}, u32[]{:S(2)}) async-start(bf16[8,128,128]{2,1,0:T(8,128)(2,1)} %gated.1), calls=%async_computation.3 | async-start | bytes 524288 | tf_op jit(solution)/shard_map/all_to_all | solution.py:533
  87.9 5.9 %all-to-all-done.3 = bf16[8,128,128]{2,1,0:T(8,128)(2,1)S(1)} async-done(((bf16[8,128,128]{2,1,0:T(8,128)(2,1)}), bf16[8,128,128]{2,1,0:T(8,128)(2,1)S(1)}, u32[]{:S(2)}, u32[]{:S(2)}) %all-to-all-start.3) | async-done | bytes 262176 | tf_op jit(solution)/shard_map/all_to_all | solution.py:533
  93.8 9.4 %all-gather = bf16[16,128,128]{2,1,0:T(8,128)(2,1)S(1)} all-gather(bf16[8,128,128]{2,1,0:T(8,128)(2,1)S(1)} %all-to-all-done.3), channel_id=2, replica_groups=mesh['zb'=8,'zr'=2,'ya'=2,'yb'=2,'x'=4,'c'=2] {'c'}, dimensions={0}, use_global_device_ids=true | all-gather | bytes 786432 | tf_op jit(solution)/shard_map/all_gather | solution.py:534
  104.3 3.7 %middle.1 = (bf16[8,256,256]{2,1,0:T(8,128)(2,1)S(1)}, bf16[128,256]{1,0:T(8,128)(2,1)S(1)}) custom-call(s32[9]{0:T(128)S(1)} %stack.83.place_ref, bf16[2,8,128,128]{3,2,1,0:T(8,128)(2,1)S(1)} %bitcast.29, bf16[1296,256]{1,0:T(8,128)(2,1)S(1)} %fusion.1.refs_0_, bf16[1296,256]{1,0:T(8,128)(2,1)} %collective-permute-done.1.refs_1_, ...), custom_call_target="tpu_custom_call" | custom-call | tf_op jit(solution)/shard_map/middle/pallas_call | solution.py:316
  108.0 4.0 %feed_enter.1 = (bf16[2,4,128,256]{3,2,1,0:T(8,128)(2,1)S(1)}, bf16[256,352]{1,0:T(8,128)(2,1)S(1)}) custom-call(s32[1]{0:T(128)} %bitcast.core_ref, bf16[8,256,256]{2,1,0:T(8,128)(2,1)S(1)} %get-tuple-element.23.rows_ref, bf16[16,3,352,128]{3,2,1,0:T(8,128)(2,1)} %bitcast.36), custom_call_target="tpu_custom_call" | custom-call | flops 922746880 | bytes 3604480 | tf_op jit(solution)/shard_map/feed_enter/pallas_call | solution.py:412
  112.1 2.3 %collective-permute-start.8 = (bf16[2,4,128,256]{3,2,1,0:T(8,128)(2,1)S(1)}, bf16[2,4,128,256]{3,2,1,0:T(8,128)(2,1)S(1)}, u32[]{:S(2)}, u32[]{:S(2)}) collective-permute-start(bf16[2,4,128,256]{3,2,1,0:T(8,128)(2,1)S(1)} %get-tuple-element.25), channel_id=1, source_target_pairs={{0,1},{1,0},{2,3},{3,2},{4,5},{5,4},{6,7},{7,6},{8,9},{9,8},{10,11... | collective-permute-start | bytes 1572872 | tf_op jit(solution)/shard_map/ppermute | solution.py:541
  114.4 2.1 %feed_leave.1.mine_ref = f32[2,4,128,256]{3,2,1,0:T(8,128)S(1)} custom-call(s32[1]{0:T(128)} %bitcast.core_ref, bf16[256,352]{1,0:T(8,128)(2,1)S(1)} %get-tuple-element.24.hidden_ref, bf16[16,3,352,128]{3,2,1,0:T(8,128)(2,1)} %bitcast.37), custom_call_target="tpu_custom_call" | custom-call | flops 184549376 | bytes 720896 | tf_op jit(solution)/shard_map/feed_leave/pallas_call | solution.py:436
  116.6 11.9 %all_to_all.37.arrived_ref = bf16[8,128,256]{2,1,0:T(8,128)(2,1)S(1)} all-to-all(bf16[8,128,256]{2,1,0:T(8,128)(2,1)S(1)} %join.1), channel_id=1, replica_groups=mesh['zb'=8,'zr'=2,'ya'=2,'yb'=2,'x'=4,'c'=2] {'x','yb'}, dimensions={0} | all-to-all | bytes 1048576 | tf_op jit(solution)/shard_map/all_to_all | solution.py:543
  128.8 8.3 %all_to_all.38.moments_ref = f32[8,1,256]{2,1,0:T(1,128)S(1)} all-to-all(f32[8,1,256]{2,1,0:T(1,128)S(1)} %get-tuple-element.27), channel_id=1, replica_groups=mesh['zb'=8,'zr'=2,'ya'=2,'yb'=2,'x'=4,'c'=2] {'x','c'}, dimensions={0} | all-to-all | bytes 16384 | tf_op jit(solution)/shard_map/all_to_all | solution.py:553
  (68 shorter events, 6.4 us)
Async XLA Ops:
  6.5 12.7 %copy-start.5 = (bf16[128,128]{1,0:T(8,128)(2,1)S(1)}, bf16[128,128]{1,0:T(8,128)(2,1)}, u32[]{:S(2)}) copy-start(bf16[128,128]{1,0:T(8,128)(2,1)} %onward_ref.1) | copy-start | bytes 98308
  6.6 12.7 %copy-start.6 = (bf16[128,128]{1,0:T(8,128)(2,1)S(1)}, bf16[128,128]{1,0:T(8,128)(2,1)}, u32[]{:S(2)}) copy-start(bf16[128,128]{1,0:T(8,128)(2,1)} %reverse_ref.1) | copy-start | bytes 98308
  6.6 14.6 %copy-start.14 = (bf16[128,256]{1,0:T(8,128)(2,1)S(1)}, bf16[128,256]{1,0:T(8,128)(2,1)}, u32[]{:S(2)}) copy-start(bf16[128,256]{1,0:T(8,128)(2,1)} %param.27) | copy-start | bytes 196612
  6.6 16.8 %copy-start.15 = (f32[256]{0:T(256)S(1)}, f32[256]{0:T(256)}, u32[]{:S(2)}) copy-start(f32[256]{0:T(256)} %param.29) | copy-start | bytes 3076
  6.6 16.8 %copy-start.16 = (f32[256]{0:T(256)S(1)}, f32[256]{0:T(256)}, u32[]{:S(2)}) copy-start(f32[256]{0:T(256)} %param.30) | copy-start | bytes 3076
  6.6 101.4 %all-gather.3.cloned.1.call-start = ((), (), s32[]{:S(2)}) async-start(), calls=%async_computation.7 | async-start | bytes 4595712 | tf_op jit(solution)/shard_map/all_gather | solution.py:238
  7.6 18.6 %copy-start.13 = (bf16[1024,256]{1,0:T(8,128)(2,1)S(1)}, bf16[1024,256]{1,0:T(8,128)(2,1)}, u32[]{:S(2)}) copy-start(bf16[1024,256]{1,0:T(8,128)(2,1)} %param.28) | copy-start | bytes 1572868
  19.1 64.0 %copy-start.2 = (bf16[128,128]{1,0:T(8,128)(2,1)S(1)}, bf16[128,128]{1,0:T(8,128)(2,1)}, u32[]{:S(2)}) copy-start(bf16[128,128]{1,0:T(8,128)(2,1)} %gate_ref.1) | copy-start | bytes 98308
  19.1 64.0 %copy-start.12 = (f32[128]{0:T(128)S(1)}, f32[128]{0:T(128)}, u32[]{:S(2)}) copy-start(f32[128]{0:T(128)} %param.26) | copy-start | bytes 1540
  21.2 5.0 %collective-permute-start = (bf16[128,256]{1,0:T(8,128)(2,1)S(1)}, bf16[128,256]{1,0:T(8,128)(2,1)S(1)}, u32[]{:S(2)}, u32[]{:S(2)}) collective-permute-start(bf16[128,256]{1,0:T(8,128)(2,1)S(1)} %copy-done.14), channel_id=1, source_target_pairs={{0,8},{8,0},{1,9},{9,1},{2,10},{10,2},{3,11},{11,3},{4,12},{12,4},... | collective-permute-start | bytes 196616 | tf_op jit(solution)/shard_map/ppermute | solution.py:255
  26.3 42.5 %collective-permute-start.2 = (bf16[1296,256]{1,0:T(8,128)(2,1)S(1)}, bf16[1296,256]{1,0:T(8,128)(2,1)S(1)}, u32[]{:S(2)}, u32[]{:S(2)}) collective-permute-start(bf16[1296,256]{1,0:T(8,128)(2,1)S(1)} %fusion.1.refs_0_), channel_id=1, source_target_pairs={{0,2},{2,4},{4,6},{6,0},{1,3},{3,5},{5,7},{7,1},{8,10},{10,12},{12... | collective-permute-start | bytes 1990664 | tf_op jit(solution)/shard_map/ppermute | solution.py:268
  29.6 41.2 %collective-permute-start.4 = (bf16[1296,256]{1,0:T(8,128)(2,1)S(1)}, bf16[1296,256]{1,0:T(8,128)(2,1)S(1)}, u32[]{:S(2)}, u32[]{:S(2)}) collective-permute-start(bf16[1296,256]{1,0:T(8,128)(2,1)S(1)} %fusion.1.refs_0_), channel_id=1, source_target_pairs={{0,4},{2,6},{4,0},{6,2},{1,5},{3,7},{5,1},{7,3},{8,12},{10,14},{12... | collective-permute-start | bytes 1990664 | tf_op jit(solution)/shard_map/ppermute | solution.py:268
  33.9 39.2 %collective-permute-start.6 = (bf16[1296,256]{1,0:T(8,128)(2,1)S(1)}, bf16[1296,256]{1,0:T(8,128)(2,1)S(1)}, u32[]{:S(2)}, u32[]{:S(2)}) collective-permute-start(bf16[1296,256]{1,0:T(8,128)(2,1)S(1)} %fusion.1.refs_0_), channel_id=1, source_target_pairs={{0,6},{2,0},{4,2},{6,4},{1,7},{3,1},{5,3},{7,5},{8,14},{10,8},{12,... | collective-permute-start | bytes 1990664 | tf_op jit(solution)/shard_map/ppermute | solution.py:268
  37.0 9.5 %all-to-all-start = ((bf16[8,40,128]{2,1,0:T(8,128)(2,1)}), bf16[8,40,128]{2,1,0:T(8,128)(2,1)S(1)}, u32[]{:S(2)}, u32[]{:S(2)}) async-start(bf16[8,40,128]{2,1,0:T(8,128)(2,1)} %get-tuple-element.18), calls=%async_computation | async-start | bytes 163840 | tf_op jit(solution)/shard_map/all_to_all | solution.py:170
  47.2 27.9 %all-to-all-start.1 = ((bf16[8,24,128]{2,1,0:T(8,128)(2,1)}), bf16[8,24,128]{2,1,0:T(8,128)(2,1)S(1)}, u32[]{:S(2)}, u32[]{:S(2)}) async-start(bf16[8,24,128]{2,1,0:T(8,128)(2,1)} %plane.1), calls=%async_computation.1 | async-start | bytes 98304 | tf_op jit(solution)/shard_map/all_to_all | solution.py:180
  61.5 41.7 %collective-permute-start.1 = (bf16[1296,256]{1,0:T(8,128)(2,1)S(1)}, bf16[1296,256]{1,0:T(8,128)(2,1)}, u32[]{:S(2)}, u32[]{:S(2)}) collective-permute-start(bf16[1296,256]{1,0:T(8,128)(2,1)S(1)} %fusion.1.refs_0_), channel_id=1, source_target_pairs={{0,1},{1,0},{2,3},{3,2},{4,5},{5,4},{6,7},{7,6},{8,9},{9,8},{10,11... | collective-permute-start | bytes 1990664 | tf_op jit(solution)/shard_map/ppermute | solution.py:537
  68.8 34.4 %collective-permute-start.3 = (bf16[1296,256]{1,0:T(8,128)(2,1)S(1)}, bf16[1296,256]{1,0:T(8,128)(2,1)}, u32[]{:S(2)}, u32[]{:S(2)}) collective-permute-start(bf16[1296,256]{1,0:T(8,128)(2,1)S(1)} %collective-permute-done.2.refs_2_), channel_id=1, source_target_pairs={{0,1},{1,0},{2,3},{3,2},{4,5},{5,4},{6,7},{7,6},{8,9},{9,8},{10,11... | collective-permute-start | bytes 1990664 | tf_op jit(solution)/shard_map/ppermute | solution.py:537
  70.7 32.5 %collective-permute-start.5 = (bf16[1296,256]{1,0:T(8,128)(2,1)S(1)}, bf16[1296,256]{1,0:T(8,128)(2,1)}, u32[]{:S(2)}, u32[]{:S(2)}) collective-permute-start(bf16[1296,256]{1,0:T(8,128)(2,1)S(1)} %collective-permute-done.4.refs_4_), channel_id=1, source_target_pairs={{0,1},{1,0},{2,3},{3,2},{4,5},{5,4},{6,7},{7,6},{8,9},{9,8},{10,11... | collective-permute-start | bytes 1990664 | tf_op jit(solution)/shard_map/ppermute | solution.py:537
  73.2 30.1 %copy-start = (bf16[1296,256]{1,0:T(8,128)(2,1)}, bf16[1296,256]{1,0:T(8,128)(2,1)S(1)}, u32[]{:S(2)}) copy-start(bf16[1296,256]{1,0:T(8,128)(2,1)S(1)} %collective-permute-done.6.refs_6_) | copy-start | bytes 1990660
  73.2 30.0 %collective-permute-start.7 = (bf16[1296,256]{1,0:T(8,128)(2,1)S(1)}, bf16[1296,256]{1,0:T(8,128)(2,1)}, u32[]{:S(2)}, u32[]{:S(2)}) collective-permute-start(bf16[1296,256]{1,0:T(8,128)(2,1)S(1)} %collective-permute-done.6.refs_6_), channel_id=1, source_target_pairs={{0,1},{1,0},{2,3},{3,2},{4,5},{5,4},{6,7},{7,6},{8,9},{9,8},{10,11... | collective-permute-start | bytes 1990664 | tf_op jit(solution)/shard_map/ppermute | solution.py:537
  84.3 9.5 %all-to-all-start.3 = ((bf16[8,128,128]{2,1,0:T(8,128)(2,1)}), bf16[8,128,128]{2,1,0:T(8,128)(2,1)S(1)}, u32[]{:S(2)}, u32[]{:S(2)}) async-start(bf16[8,128,128]{2,1,0:T(8,128)(2,1)} %gated.1), calls=%async_computation.3 | async-start | bytes 524288 | tf_op jit(solution)/shard_map/all_to_all | solution.py:533
  112.1 4.4 %collective-permute-start.8 = (bf16[2,4,128,256]{3,2,1,0:T(8,128)(2,1)S(1)}, bf16[2,4,128,256]{3,2,1,0:T(8,128)(2,1)S(1)}, u32[]{:S(2)}, u32[]{:S(2)}) collective-permute-start(bf16[2,4,128,256]{3,2,1,0:T(8,128)(2,1)S(1)} %get-tuple-element.25), channel_id=1, source_target_pairs={{0,1},{1,0},{2,3},{3,2},{4,5},{5,4},{6,7},{7,6},{8,9},{9,8},{10,11... | collective-permute-start | bytes 1572872 | tf_op jit(solution)/shard_map/ppermute | solution.py:541
  116.6 20.5 %copy-start.7 = (f32[256]{0:T(256)S(1)}, f32[256]{0:T(256)}, u32[]{:S(2)}) copy-start(f32[256]{0:T(256)} %param.34) | copy-start | bytes 3076
  116.6 20.4 %copy-start.8 = (f32[256]{0:T(256)S(1)}, f32[256]{0:T(256)}, u32[]{:S(2)}) copy-start(f32[256]{0:T(256)} %param.35) | copy-start | bytes 3076
  (6 other events, 64.3 us)
Sparse Core Ops, SparseCore 0:
  19.3 75.1 all-gather.2
where the time goes:
time: 146 us; the launch traced here: 145 us
  starting transfers between devices  50.1 us (34%)
  blocking collectives  48.1 us (33%)
  Pallas kernels  15.6 us (11%)
  waiting for transfers between devices  14.4 us (10%)
  between operations  14 us (10%)
    all_to_all x1, starting transfers between devices, states_around(): others, = near(lax.all_to_all(totals, 'zb', 0, 0, tiled=True))  14.3 us
    ppermute x4, starting transfers between devices, layer(): both += [block, lax.ppermute(block, 'c', SWAP)]  13.5 us
    all_to_all x1, blocking collectives, layer(): shares = lax.all_to_all(joined(mine, other), ('x', 'yb'), 0, 0, tiled=True)  11.9 us
    ppermute x3, starting transfers between devices, spread_over_x(): lax.ppermute(block, 'x', [(i, (i + k) % count) for i in range(count)])  10.7 us
    all_to_all x1, blocking collectives, gathered_weights(): lax.all_to_all(jnp.stack(halves + halves), ('ya', 'yb'), 0, 0, tiled=True)  10.5 us
    all_gather x1, blocking collectives, layer(): everyone = lax.all_gather(everyone, 'c')  9.39 us
    all_to_all x1, blocking collectives, layer(): moments = lax.all_to_all(moments, TP, 0, 0, tiled=True)  8.31 us
    all_to_all x1, blocking collectives, states_around(): return lax.all_to_all(before, NEAR, 0, 0, tiled=True)  7.96 us
  transfers between devices with their start and end apart: 13, of which 3 were waited for; matrix products, arithmetic and copies ran while one was open for 0% of the time, Pallas kernels for 7%

commit v1 on v0

--- a/solution.py
+++ b/solution.py
@@ -219,10 +219,17 @@
 ANY = pl.BlockSpec(memory_space=pl.ANY)
 
 
-def turn_kernel(in_ref, out_ref):
+def turn_kernel(in_ref, out_ref, turned_ref, sem_ref):
+    copies = []
     for kind in range(3):
         rows = jnp.concatenate([in_ref[y, kind] for y in range(4)], axis=0)
-        out_ref[kind] = rows.T
+        turned_ref[kind] = rows.T
+        copies.append(
+            pltpu.make_async_copy(turned_ref.at[kind], out_ref.at[kind], sem_ref.at[kind])
+        )
+        copies[kind].start()
+    for copy in copies:
+        copy.wait()
 
 
 def gathered_weights(gate, up, down):
@@ -232,6 +239,12 @@
     shard = pl.pallas_call(
         turn_kernel,
         out_shape=jax.ShapeDtypeStruct((3, HALF, 128), jnp.bfloat16),
+        in_specs=[VMEM],
+        out_specs=ANY,
+        scratch_shapes=[
+            pltpu.VMEM((3, HALF, 128), jnp.bfloat16),
+            pltpu.SemaphoreType.DMA((3,)),
+        ],
         compiler_params=pltpu.CompilerParams(vmem_limit_bytes=6 << 20),
         name="turn",
     )(*near(arrived)).reshape(3 * HALF, 128)
@@ -404,7 +417,7 @@
     for pair in range(2):
         for s in range(4):
             total = mine_ref[pair, s] + other_ref[pair, s].astype(jnp.float32)
-            out_ref[2 * s + pair] = total.astype(jnp.bfloat16)
+            out_ref[4 * pair + s] = total.astype(jnp.bfloat16)
 
 
 def feed_enter(core, rows, weights):
@@ -540,7 +553,7 @@
     send, hidden = feed_enter(core, middle, weights)
     other = lax.ppermute(send, "c", SWAP)
     mine = feed_leave(core, hidden, weights)
-    shares = lax.all_to_all(joined(mine, other), ("x", "yb"), 0, 0, tiled=True)
+    shares = lax.all_to_all(joined(mine, other), ("yb", "x"), 0, 0, tiled=True)
     before_final, moments = pl.pallas_call(
         total_kernel,
         out_shape=[

time: 146 us -> 146 us (level)
  no operation moved by 1% of the time
where the time goes in v1:
time: 146 us; the launch traced here: 145 us
  starting transfers between devices  50.1 us (34%)
  blocking collectives  48.3 us (33%)
  Pallas kernels  15.6 us (11%)
  waiting for transfers between devices  14.5 us (10%)
  between operations  14 us (10%)
    all_to_all x1, starting transfers between devices, states_around(): others, = near(lax.all_to_all(totals, 'zb', 0, 0, tiled=True))  14.3 us
    ppermute x4, starting transfers between devices, layer(): both += [block, lax.ppermute(block, 'c', SWAP)]  13.6 us
    all_to_all x1, blocking collectives, layer(): shares = lax.all_to_all(joined(mine, other), ('yb', 'x'), 0, 0, tiled=True)  12.6 us
    ppermute x3, starting transfers between devices, spread_over_x(): lax.ppermute(block, 'x', [(i, (i + k) % count) for i in range(count)])  10.7 us
    all_to_all x1, blocking collectives, gathered_weights(): lax.all_to_all(jnp.stack(halves + halves), ('ya', 'yb'), 0, 0, tiled=True)  10.5 us
    all_gather x1, blocking collectives, layer(): everyone = lax.all_gather(everyone, 'c')  9.68 us
    all_to_all x1, blocking collectives, layer(): moments = lax.all_to_all(moments, TP, 0, 0, tiled=True)  7.78 us
    all_to_all x1, blocking collectives, states_around(): return lax.all_to_all(before, NEAR, 0, 0, tiled=True)  7.7 us
  transfers between devices with their start and end apart: 13, of which 3 were waited for; matrix products, arithmetic and copies ran while one was open for 0% of the time, Pallas kernels for 7%

profile of v1, /device:TPU:1, one launch (start us, length us, event | category | flops | bytes accessed | tf_op | source)
XLA Modules:
  0.0 144.9 jit_solution(7907180338598283544)
XLA Ops:
  7.8 10.5 %all_to_all.35.in_ref = bf16[4,3,32,352]{3,2,1,0:T(8,128)(2,1)S(1)} all-to-all(bf16[4,3,32,352]{3,2,1,0:T(8,128)(2,1)S(1)} %pad_maximum_fusion), channel_id=1, replica_groups=mesh['zb'=8,'zr'=2,'ya'=2,'yb'=2,'x'=4,'c'=2] {'ya','yb'}, dimensions={0} | all-to-all | bytes 540672 | tf_op jit(solution)/shard_map/all_to_all | solution.py:238
  19.2 2.0 %local.1 = (f32[128,128]{1,0:T(8,128)S(1)}, f32[128,256]{1,0:T(8,128)S(1)}, bf16[8,40,128]{2,1,0:T(8,128)(2,1)}) custom-call(bf16[128,128]{1,0:T(8,128)(2,1)S(1)} %copy-done.3, bf16[128,128]{1,0:T(8,128)(2,1)S(1)} %copy-done.4, bf16[128,128]{1,0:T(8,128)(2,1)S(1)} %copy-done.5, bf16[128,128]{1,0:T(8,128)(2,1)S(1)} %copy-done.6, f32[1,128]{1,0:T(1,128)S(1)} %bitcast.32, ...), custom_call_target="tpu_custom_call" | custom-call | tf_op jit(solution)/shard_map/local/pallas_call | solution.py:92
  21.2 2.2 %collective-permute-start = (bf16[128,256]{1,0:T(8,128)(2,1)S(1)}, bf16[128,256]{1,0:T(8,128)(2,1)S(1)}, u32[]{:S(2)}, u32[]{:S(2)}) collective-permute-start(bf16[128,256]{1,0:T(8,128)(2,1)S(1)} %copy-done.14), channel_id=1, source_target_pairs={{0,8},{8,0},{1,9},{9,1},{2,10},{10,2},{3,11},{11,3},{4,12},{12,4},... | collective-permute-start | bytes 196616 | tf_op jit(solution)/shard_map/ppermute | solution.py:268
  23.6 2.6 %collective-permute-done = bf16[128,256]{1,0:T(8,128)(2,1)S(1)} collective-permute-done((bf16[128,256]{1,0:T(8,128)(2,1)S(1)}, bf16[128,256]{1,0:T(8,128)(2,1)S(1)}, u32[]{:S(2)}, u32[]{:S(2)}) %collective-permute-start) | collective-permute-done | bytes 65568 | tf_op jit(solution)/shard_map/ppermute | solution.py:268
  26.3 3.3 %collective-permute-start.2 = (bf16[1296,256]{1,0:T(8,128)(2,1)S(1)}, bf16[1296,256]{1,0:T(8,128)(2,1)S(1)}, u32[]{:S(2)}, u32[]{:S(2)}) collective-permute-start(bf16[1296,256]{1,0:T(8,128)(2,1)S(1)} %fusion.1.refs_0_), channel_id=1, source_target_pairs={{0,2},{2,4},{4,6},{6,0},{1,3},{3,5},{5,7},{7,1},{8,10},{10,12},{12... | collective-permute-start | bytes 1990664 | tf_op jit(solution)/shard_map/ppermute | solution.py:281
  29.6 4.4 %collective-permute-start.4 = (bf16[1296,256]{1,0:T(8,128)(2,1)S(1)}, bf16[1296,256]{1,0:T(8,128)(2,1)S(1)}, u32[]{:S(2)}, u32[]{:S(2)}) collective-permute-start(bf16[1296,256]{1,0:T(8,128)(2,1)S(1)} %fusion.1.refs_0_), channel_id=1, source_target_pairs={{0,4},{2,6},{4,0},{6,2},{1,5},{3,7},{5,1},{7,3},{8,12},{10,14},{12... | collective-permute-start | bytes 1990664 | tf_op jit(solution)/shard_map/ppermute | solution.py:281
  33.9 3.1 %collective-permute-start.6 = (bf16[1296,256]{1,0:T(8,128)(2,1)S(1)}, bf16[1296,256]{1,0:T(8,128)(2,1)S(1)}, u32[]{:S(2)}, u32[]{:S(2)}) collective-permute-start(bf16[1296,256]{1,0:T(8,128)(2,1)S(1)} %fusion.1.refs_0_), channel_id=1, source_target_pairs={{0,6},{2,0},{4,2},{6,4},{1,7},{3,1},{5,3},{7,5},{8,14},{10,8},{12,... | collective-permute-start | bytes 1990664 | tf_op jit(solution)/shard_map/ppermute | solution.py:281
  37.0 3.7 %all-to-all-start = ((bf16[8,40,128]{2,1,0:T(8,128)(2,1)}), bf16[8,40,128]{2,1,0:T(8,128)(2,1)S(1)}, u32[]{:S(2)}, u32[]{:S(2)}) async-start(bf16[8,40,128]{2,1,0:T(8,128)(2,1)} %get-tuple-element.18), calls=%async_computation | async-start | bytes 163840 | tf_op jit(solution)/shard_map/all_to_all | solution.py:170
  40.7 5.8 %all-to-all-done.arrived_ref = bf16[8,40,128]{2,1,0:T(8,128)(2,1)S(1)} async-done(((bf16[8,40,128]{2,1,0:T(8,128)(2,1)}), bf16[8,40,128]{2,1,0:T(8,128)(2,1)S(1)}, u32[]{:S(2)}, u32[]{:S(2)}) %all-to-all-start) | async-done | bytes 81952 | tf_op jit(solution)/shard_map/all_to_all | solution.py:170
  47.2 14.3 %all-to-all-start.1 = ((bf16[8,24,128]{2,1,0:T(8,128)(2,1)}), bf16[8,24,128]{2,1,0:T(8,128)(2,1)S(1)}, u32[]{:S(2)}, u32[]{:S(2)}) async-start(bf16[8,24,128]{2,1,0:T(8,128)(2,1)} %plane.1), calls=%async_computation.1 | async-start | bytes 98304 | tf_op jit(solution)/shard_map/all_to_all | solution.py:180
  61.5 7.3 %collective-permute-start.1 = (bf16[1296,256]{1,0:T(8,128)(2,1)S(1)}, bf16[1296,256]{1,0:T(8,128)(2,1)}, u32[]{:S(2)}, u32[]{:S(2)}) collective-permute-start(bf16[1296,256]{1,0:T(8,128)(2,1)S(1)} %fusion.1.refs_0_), channel_id=1, source_target_pairs={{0,1},{1,0},{2,3},{3,2},{4,5},{5,4},{6,7},{7,6},{8,9},{9,8},{10,11... | collective-permute-start | bytes 1990664 | tf_op jit(solution)/shard_map/ppermute | solution.py:550
  68.8 1.9 %collective-permute-start.3 = (bf16[1296,256]{1,0:T(8,128)(2,1)S(1)}, bf16[1296,256]{1,0:T(8,128)(2,1)}, u32[]{:S(2)}, u32[]{:S(2)}) collective-permute-start(bf16[1296,256]{1,0:T(8,128)(2,1)S(1)} %collective-permute-done.2.refs_2_), channel_id=1, source_target_pairs={{0,1},{1,0},{2,3},{3,2},{4,5},{5,4},{6,7},{7,6},{8,9},{9,8},{10,11... | collective-permute-start | bytes 1990664 | tf_op jit(solution)/shard_map/ppermute | solution.py:550
  70.8 2.4 %collective-permute-start.5 = (bf16[1296,256]{1,0:T(8,128)(2,1)S(1)}, bf16[1296,256]{1,0:T(8,128)(2,1)}, u32[]{:S(2)}, u32[]{:S(2)}) collective-permute-start(bf16[1296,256]{1,0:T(8,128)(2,1)S(1)} %collective-permute-done.4.refs_4_), channel_id=1, source_target_pairs={{0,1},{1,0},{2,3},{3,2},{4,5},{5,4},{6,7},{7,6},{8,9},{9,8},{10,11... | collective-permute-start | bytes 1990664 | tf_op jit(solution)/shard_map/ppermute | solution.py:550
  73.2 1.9 %collective-permute-start.7 = (bf16[1296,256]{1,0:T(8,128)(2,1)S(1)}, bf16[1296,256]{1,0:T(8,128)(2,1)}, u32[]{:S(2)}, u32[]{:S(2)}) collective-permute-start(bf16[1296,256]{1,0:T(8,128)(2,1)S(1)} %collective-permute-done.6.refs_6_), channel_id=1, source_target_pairs={{0,1},{1,0},{2,3},{3,2},{4,5},{5,4},{6,7},{7,6},{8,9},{9,8},{10,11... | collective-permute-start | bytes 1990664 | tf_op jit(solution)/shard_map/ppermute | solution.py:550
  75.2 7.7 %all_to_all.36.back_ref = bf16[8,32,128]{2,1,0:T(8,128)(2,1)S(1)} all-to-all(bf16[8,32,128]{2,1,0:T(8,128)(2,1)S(1)} %before.1), channel_id=1, replica_groups=mesh['zb'=8,'zr'=2,'ya'=2,'yb'=2,'x'=4,'c'=2] {'zr','ya','yb'}, dimensions={0} | all-to-all | bytes 131072 | tf_op jit(solution)/shard_map/all_to_all | solution.py:189
  84.1 3.4 %all-to-all-start.3 = ((bf16[8,128,128]{2,1,0:T(8,128)(2,1)}), bf16[8,128,128]{2,1,0:T(8,128)(2,1)S(1)}, u32[]{:S(2)}, u32[]{:S(2)}) async-start(bf16[8,128,128]{2,1,0:T(8,128)(2,1)} %gated.1), calls=%async_computation.3 | async-start | bytes 524288 | tf_op jit(solution)/shard_map/all_to_all | solution.py:546
  87.7 5.9 %all-to-all-done.3 = bf16[8,128,128]{2,1,0:T(8,128)(2,1)S(1)} async-done(((bf16[8,128,128]{2,1,0:T(8,128)(2,1)}), bf16[8,128,128]{2,1,0:T(8,128)(2,1)S(1)}, u32[]{:S(2)}, u32[]{:S(2)}) %all-to-all-start.3) | async-done | bytes 262176 | tf_op jit(solution)/shard_map/all_to_all | solution.py:546
  93.6 9.7 %all-gather = bf16[16,128,128]{2,1,0:T(8,128)(2,1)S(1)} all-gather(bf16[8,128,128]{2,1,0:T(8,128)(2,1)S(1)} %all-to-all-done.3), channel_id=2, replica_groups=mesh['zb'=8,'zr'=2,'ya'=2,'yb'=2,'x'=4,'c'=2] {'c'}, dimensions={0}, use_global_device_ids=true | all-gather | bytes 786432 | tf_op jit(solution)/shard_map/all_gather | solution.py:547
  104.4 3.7 %middle.1 = (bf16[8,256,256]{2,1,0:T(8,128)(2,1)S(1)}, bf16[128,256]{1,0:T(8,128)(2,1)S(1)}) custom-call(s32[9]{0:T(128)S(1)} %stack.83.place_ref, bf16[2,8,128,128]{3,2,1,0:T(8,128)(2,1)S(1)} %bitcast.29, bf16[1296,256]{1,0:T(8,128)(2,1)S(1)} %fusion.1.refs_0_, bf16[1296,256]{1,0:T(8,128)(2,1)} %collective-permute-done.1.refs_1_, ...), custom_call_target="tpu_custom_call" | custom-call | tf_op jit(solution)/shard_map/middle/pallas_call | solution.py:329
  108.1 4.0 %feed_enter.1 = (bf16[2,4,128,256]{3,2,1,0:T(8,128)(2,1)S(1)}, bf16[256,352]{1,0:T(8,128)(2,1)S(1)}) custom-call(s32[1]{0:T(128)} %bitcast.core_ref, bf16[8,256,256]{2,1,0:T(8,128)(2,1)S(1)} %get-tuple-element.23.rows_ref, bf16[16,3,352,128]{3,2,1,0:T(8,128)(2,1)} %bitcast.36), custom_call_target="tpu_custom_call" | custom-call | flops 922746880 | bytes 3604480 | tf_op jit(solution)/shard_map/feed_enter/pallas_call | solution.py:425
  112.2 2.3 %collective-permute-start.8 = (bf16[2,4,128,256]{3,2,1,0:T(8,128)(2,1)S(1)}, bf16[2,4,128,256]{3,2,1,0:T(8,128)(2,1)S(1)}, u32[]{:S(2)}, u32[]{:S(2)}) collective-permute-start(bf16[2,4,128,256]{3,2,1,0:T(8,128)(2,1)S(1)} %get-tuple-element.25), channel_id=1, source_target_pairs={{0,1},{1,0},{2,3},{3,2},{4,5},{5,4},{6,7},{7,6},{8,9},{9,8},{10,11... | collective-permute-start | bytes 1572872 | tf_op jit(solution)/shard_map/ppermute | solution.py:554
  114.5 2.1 %feed_leave.1.mine_ref = f32[2,4,128,256]{3,2,1,0:T(8,128)S(1)} custom-call(s32[1]{0:T(128)} %bitcast.core_ref, bf16[256,352]{1,0:T(8,128)(2,1)S(1)} %get-tuple-element.24.hidden_ref, bf16[16,3,352,128]{3,2,1,0:T(8,128)(2,1)} %bitcast.37), custom_call_target="tpu_custom_call" | custom-call | flops 184549376 | bytes 720896 | tf_op jit(solution)/shard_map/feed_leave/pallas_call | solution.py:449
  116.7 12.6 %all_to_all.37.arrived_ref = bf16[8,128,256]{2,1,0:T(8,128)(2,1)S(1)} all-to-all(bf16[8,128,256]{2,1,0:T(8,128)(2,1)S(1)} %join.1), channel_id=1, replica_groups=mesh['zb'=8,'zr'=2,'ya'=2,'yb'=2,'x'=4,'c'=2] {'yb','x'}, dimensions={0} | all-to-all | bytes 1048576 | tf_op jit(solution)/shard_map/all_to_all | solution.py:556
  129.6 7.8 %all_to_all.38.moments_ref = f32[8,1,256]{2,1,0:T(1,128)S(1)} all-to-all(f32[8,1,256]{2,1,0:T(1,128)S(1)} %get-tuple-element.27), channel_id=1, replica_groups=mesh['zb'=8,'zr'=2,'ya'=2,'yb'=2,'x'=4,'c'=2] {'x','c'}, dimensions={0} | all-to-all | bytes 16384 | tf_op jit(solution)/shard_map/all_to_all | solution.py:566
  (68 shorter events, 6.4 us)
Async XLA Ops:
  6.5 12.7 %copy-start.5 = (bf16[128,128]{1,0:T(8,128)(2,1)S(1)}, bf16[128,128]{1,0:T(8,128)(2,1)}, u32[]{:S(2)}) copy-start(bf16[128,128]{1,0:T(8,128)(2,1)} %onward_ref.1) | copy-start | bytes 98308
  6.6 12.7 %copy-start.6 = (bf16[128,128]{1,0:T(8,128)(2,1)S(1)}, bf16[128,128]{1,0:T(8,128)(2,1)}, u32[]{:S(2)}) copy-start(bf16[128,128]{1,0:T(8,128)(2,1)} %reverse_ref.1) | copy-start | bytes 98308
  6.6 14.6 %copy-start.14 = (bf16[128,256]{1,0:T(8,128)(2,1)S(1)}, bf16[128,256]{1,0:T(8,128)(2,1)}, u32[]{:S(2)}) copy-start(bf16[128,256]{1,0:T(8,128)(2,1)} %param.27) | copy-start | bytes 196612
  6.6 16.8 %copy-start.15 = (f32[256]{0:T(256)S(1)}, f32[256]{0:T(256)}, u32[]{:S(2)}) copy-start(f32[256]{0:T(256)} %param.29) | copy-start | bytes 3076
  6.6 16.8 %copy-start.16 = (f32[256]{0:T(256)S(1)}, f32[256]{0:T(256)}, u32[]{:S(2)}) copy-start(f32[256]{0:T(256)} %param.30) | copy-start | bytes 3076
  6.6 101.5 %all-gather.3.cloned.1.call-start = ((), (), s32[]{:S(2)}) async-start(), calls=%async_computation.7 | async-start | bytes 4595712 | tf_op jit(solution)/shard_map/all_gather | solution.py:251
  7.6 18.6 %copy-start.13 = (bf16[1024,256]{1,0:T(8,128)(2,1)S(1)}, bf16[1024,256]{1,0:T(8,128)(2,1)}, u32[]{:S(2)}) copy-start(bf16[1024,256]{1,0:T(8,128)(2,1)} %param.28) | copy-start | bytes 1572868
  19.1 63.8 %copy-start.2 = (bf16[128,128]{1,0:T(8,128)(2,1)S(1)}, bf16[128,128]{1,0:T(8,128)(2,1)}, u32[]{:S(2)}) copy-start(bf16[128,128]{1,0:T(8,128)(2,1)} %gate_ref.1) | copy-start | bytes 98308
  19.1 63.8 %copy-start.12 = (f32[128]{0:T(128)S(1)}, f32[128]{0:T(128)}, u32[]{:S(2)}) copy-start(f32[128]{0:T(128)} %param.26) | copy-start | bytes 1540
  21.2 5.0 %collective-permute-start = (bf16[128,256]{1,0:T(8,128)(2,1)S(1)}, bf16[128,256]{1,0:T(8,128)(2,1)S(1)}, u32[]{:S(2)}, u32[]{:S(2)}) collective-permute-start(bf16[128,256]{1,0:T(8,128)(2,1)S(1)} %copy-done.14), channel_id=1, source_target_pairs={{0,8},{8,0},{1,9},{9,1},{2,10},{10,2},{3,11},{11,3},{4,12},{12,4},... | collective-permute-start | bytes 196616 | tf_op jit(solution)/shard_map/ppermute | solution.py:268
  26.3 42.5 %collective-permute-start.2 = (bf16[1296,256]{1,0:T(8,128)(2,1)S(1)}, bf16[1296,256]{1,0:T(8,128)(2,1)S(1)}, u32[]{:S(2)}, u32[]{:S(2)}) collective-permute-start(bf16[1296,256]{1,0:T(8,128)(2,1)S(1)} %fusion.1.refs_0_), channel_id=1, source_target_pairs={{0,2},{2,4},{4,6},{6,0},{1,3},{3,5},{5,7},{7,1},{8,10},{10,12},{12... | collective-permute-start | bytes 1990664 | tf_op jit(solution)/shard_map/ppermute | solution.py:281
  29.6 41.2 %collective-permute-start.4 = (bf16[1296,256]{1,0:T(8,128)(2,1)S(1)}, bf16[1296,256]{1,0:T(8,128)(2,1)S(1)}, u32[]{:S(2)}, u32[]{:S(2)}) collective-permute-start(bf16[1296,256]{1,0:T(8,128)(2,1)S(1)} %fusion.1.refs_0_), channel_id=1, source_target_pairs={{0,4},{2,6},{4,0},{6,2},{1,5},{3,7},{5,1},{7,3},{8,12},{10,14},{12... | collective-permute-start | bytes 1990664 | tf_op jit(solution)/shard_map/ppermute | solution.py:281
  33.9 39.2 %collective-permute-start.6 = (bf16[1296,256]{1,0:T(8,128)(2,1)S(1)}, bf16[1296,256]{1,0:T(8,128)(2,1)S(1)}, u32[]{:S(2)}, u32[]{:S(2)}) collective-permute-start(bf16[1296,256]{1,0:T(8,128)(2,1)S(1)} %fusion.1.refs_0_), channel_id=1, source_target_pairs={{0,6},{2,0},{4,2},{6,4},{1,7},{3,1},{5,3},{7,5},{8,14},{10,8},{12,... | collective-permute-start | bytes 1990664 | tf_op jit(solution)/shard_map/ppermute | solution.py:281
  37.0 9.5 %all-to-all-start = ((bf16[8,40,128]{2,1,0:T(8,128)(2,1)}), bf16[8,40,128]{2,1,0:T(8,128)(2,1)S(1)}, u32[]{:S(2)}, u32[]{:S(2)}) async-start(bf16[8,40,128]{2,1,0:T(8,128)(2,1)} %get-tuple-element.18), calls=%async_computation | async-start | bytes 163840 | tf_op jit(solution)/shard_map/all_to_all | solution.py:170
  47.2 27.9 %all-to-all-start.1 = ((bf16[8,24,128]{2,1,0:T(8,128)(2,1)}), bf16[8,24,128]{2,1,0:T(8,128)(2,1)S(1)}, u32[]{:S(2)}, u32[]{:S(2)}) async-start(bf16[8,24,128]{2,1,0:T(8,128)(2,1)} %plane.1), calls=%async_computation.1 | async-start | bytes 98304 | tf_op jit(solution)/shard_map/all_to_all | solution.py:180
  61.5 41.8 %collective-permute-start.1 = (bf16[1296,256]{1,0:T(8,128)(2,1)S(1)}, bf16[1296,256]{1,0:T(8,128)(2,1)}, u32[]{:S(2)}, u32[]{:S(2)}) collective-permute-start(bf16[1296,256]{1,0:T(8,128)(2,1)S(1)} %fusion.1.refs_0_), channel_id=1, source_target_pairs={{0,1},{1,0},{2,3},{3,2},{4,5},{5,4},{6,7},{7,6},{8,9},{9,8},{10,11... | collective-permute-start | bytes 1990664 | tf_op jit(solution)/shard_map/ppermute | solution.py:550
  68.8 34.5 %collective-permute-start.3 = (bf16[1296,256]{1,0:T(8,128)(2,1)S(1)}, bf16[1296,256]{1,0:T(8,128)(2,1)}, u32[]{:S(2)}, u32[]{:S(2)}) collective-permute-start(bf16[1296,256]{1,0:T(8,128)(2,1)S(1)} %collective-permute-done.2.refs_2_), channel_id=1, source_target_pairs={{0,1},{1,0},{2,3},{3,2},{4,5},{5,4},{6,7},{7,6},{8,9},{9,8},{10,11... | collective-permute-start | bytes 1990664 | tf_op jit(solution)/shard_map/ppermute | solution.py:550
  70.8 32.6 %collective-permute-start.5 = (bf16[1296,256]{1,0:T(8,128)(2,1)S(1)}, bf16[1296,256]{1,0:T(8,128)(2,1)}, u32[]{:S(2)}, u32[]{:S(2)}) collective-permute-start(bf16[1296,256]{1,0:T(8,128)(2,1)S(1)} %collective-permute-done.4.refs_4_), channel_id=1, source_target_pairs={{0,1},{1,0},{2,3},{3,2},{4,5},{5,4},{6,7},{7,6},{8,9},{9,8},{10,11... | collective-permute-start | bytes 1990664 | tf_op jit(solution)/shard_map/ppermute | solution.py:550
  73.2 30.2 %copy-start = (bf16[1296,256]{1,0:T(8,128)(2,1)}, bf16[1296,256]{1,0:T(8,128)(2,1)S(1)}, u32[]{:S(2)}) copy-start(bf16[1296,256]{1,0:T(8,128)(2,1)S(1)} %collective-permute-done.6.refs_6_) | copy-start | bytes 1990660
  73.2 30.1 %collective-permute-start.7 = (bf16[1296,256]{1,0:T(8,128)(2,1)S(1)}, bf16[1296,256]{1,0:T(8,128)(2,1)}, u32[]{:S(2)}, u32[]{:S(2)}) collective-permute-start(bf16[1296,256]{1,0:T(8,128)(2,1)S(1)} %collective-permute-done.6.refs_6_), channel_id=1, source_target_pairs={{0,1},{1,0},{2,3},{3,2},{4,5},{5,4},{6,7},{7,6},{8,9},{9,8},{10,11... | collective-permute-start | bytes 1990664 | tf_op jit(solution)/shard_map/ppermute | solution.py:550
  84.1 9.5 %all-to-all-start.3 = ((bf16[8,128,128]{2,1,0:T(8,128)(2,1)}), bf16[8,128,128]{2,1,0:T(8,128)(2,1)S(1)}, u32[]{:S(2)}, u32[]{:S(2)}) async-start(bf16[8,128,128]{2,1,0:T(8,128)(2,1)} %gated.1), calls=%async_computation.3 | async-start | bytes 524288 | tf_op jit(solution)/shard_map/all_to_all | solution.py:546
  112.2 4.4 %collective-permute-start.8 = (bf16[2,4,128,256]{3,2,1,0:T(8,128)(2,1)S(1)}, bf16[2,4,128,256]{3,2,1,0:T(8,128)(2,1)S(1)}, u32[]{:S(2)}, u32[]{:S(2)}) collective-permute-start(bf16[2,4,128,256]{3,2,1,0:T(8,128)(2,1)S(1)} %get-tuple-element.25), channel_id=1, source_target_pairs={{0,1},{1,0},{2,3},{3,2},{4,5},{5,4},{6,7},{7,6},{8,9},{9,8},{10,11... | collective-permute-start | bytes 1572872 | tf_op jit(solution)/shard_map/ppermute | solution.py:554
  116.7 20.6 %copy-start.7 = (f32[256]{0:T(256)S(1)}, f32[256]{0:T(256)}, u32[]{:S(2)}) copy-start(f32[256]{0:T(256)} %param.34) | copy-start | bytes 3076
  116.7 20.6 %copy-start.8 = (f32[256]{0:T(256)S(1)}, f32[256]{0:T(256)}, u32[]{:S(2)}) copy-start(f32[256]{0:T(256)} %param.35) | copy-start | bytes 3076
  (6 other events, 64.3 us)
Sparse Core Ops, SparseCore 0:
  19.3 75.1 all-gather.2

commit v2 on v0

--- a/solution.py
+++ b/solution.py
@@ -362,12 +362,15 @@
             )
         )
     downs = down_copies(1 - core_ref[0], weights_ref, leave_ref, leave_sem)
-    for copy in copies + downs:
+    for copy in copies:
         copy.start()
     sums = [0.0, 0.0]
     for s in range(parts):
         x = jnp.concatenate([rows_ref[2 * s], rows_ref[2 * s + 1]], axis=1)
         copies[s].wait()
+        if s == 0:
+            for copy in downs:
+                copy.start()
         for kind in range(2):
             wide = [enter_ref[each * s + j, kind] for j in range(each)]
             sums[kind] += lax.dot_general(
@@ -404,7 +407,7 @@
     for pair in range(2):
         for s in range(4):
             total = mine_ref[pair, s] + other_ref[pair, s].astype(jnp.float32)
-            out_ref[2 * s + pair] = total.astype(jnp.bfloat16)
+            out_ref[4 * pair + s] = total.astype(jnp.bfloat16)
 
 
 def feed_enter(core, rows, weights):
@@ -540,7 +543,7 @@
     send, hidden = feed_enter(core, middle, weights)
     other = lax.ppermute(send, "c", SWAP)
     mine = feed_leave(core, hidden, weights)
-    shares = lax.all_to_all(joined(mine, other), ("x", "yb"), 0, 0, tiled=True)
+    shares = lax.all_to_all(joined(mine, other), ("yb", "x"), 0, 0, tiled=True)
     before_final, moments = pl.pallas_call(
         total_kernel,
         out_shape=[

time: 146 us -> 146 us (level)
  no operation moved by 1% of the time
where the time goes in v2:
time: 146 us; the launch traced here: 145 us
  starting transfers between devices  50.1 us (34%)
  blocking collectives  48.3 us (33%)
  Pallas kernels  15.6 us (11%)
  waiting for transfers between devices  14.4 us (10%)
  between operations  14 us (10%)
    all_to_all x1, starting transfers between devices, states_around(): others, = near(lax.all_to_all(totals, 'zb', 0, 0, tiled=True))  14.3 us
    ppermute x4, starting transfers between devices, layer(): both += [block, lax.ppermute(block, 'c', SWAP)]  13.5 us
    all_to_all x1, blocking collectives, layer(): shares = lax.all_to_all(joined(mine, other), ('yb', 'x'), 0, 0, tiled=True)  12.6 us
    ppermute x3, starting transfers between devices, spread_over_x(): lax.ppermute(block, 'x', [(i, (i + k) % count) for i in range(count)])  10.7 us
    all_to_all x1, blocking collectives, gathered_weights(): lax.all_to_all(jnp.stack(halves + halves), ('ya', 'yb'), 0, 0, tiled=True)  10.5 us
    all_gather x1, blocking collectives, layer(): everyone = lax.all_gather(everyone, 'c')  9.39 us
    all_to_all x1, blocking collectives, states_around(): return lax.all_to_all(before, NEAR, 0, 0, tiled=True)  7.96 us
    all_to_all x1, blocking collectives, layer(): moments = lax.all_to_all(moments, TP, 0, 0, tiled=True)  7.78 us
  transfers between devices with their start and end apart: 13, of which 3 were waited for; matrix products, arithmetic and copies ran while one was open for 0% of the time, Pallas kernels for 7%

profile of v2, /device:TPU:1, one launch (start us, length us, event | category | flops | bytes accessed | tf_op | source)
XLA Modules:
  0.0 144.8 jit_solution(12274452063021827045)
XLA Ops:
  7.8 10.5 %all_to_all.35.in_ref = bf16[4,3,32,352]{3,2,1,0:T(8,128)(2,1)S(1)} all-to-all(bf16[4,3,32,352]{3,2,1,0:T(8,128)(2,1)S(1)} %pad_maximum_fusion), channel_id=1, replica_groups=mesh['zb'=8,'zr'=2,'ya'=2,'yb'=2,'x'=4,'c'=2] {'ya','yb'}, dimensions={0} | all-to-all | bytes 540672 | tf_op jit(solution)/shard_map/all_to_all | solution.py:231
  19.2 2.0 %local.1 = (f32[128,128]{1,0:T(8,128)S(1)}, f32[128,256]{1,0:T(8,128)S(1)}, bf16[8,40,128]{2,1,0:T(8,128)(2,1)}) custom-call(bf16[128,128]{1,0:T(8,128)(2,1)S(1)} %copy-done.3, bf16[128,128]{1,0:T(8,128)(2,1)S(1)} %copy-done.4, bf16[128,128]{1,0:T(8,128)(2,1)S(1)} %copy-done.5, bf16[128,128]{1,0:T(8,128)(2,1)S(1)} %copy-done.6, f32[1,128]{1,0:T(1,128)S(1)} %bitcast.32, ...), custom_call_target="tpu_custom_call" | custom-call | tf_op jit(solution)/shard_map/local/pallas_call | solution.py:92
  21.2 2.2 %collective-permute-start = (bf16[128,256]{1,0:T(8,128)(2,1)S(1)}, bf16[128,256]{1,0:T(8,128)(2,1)S(1)}, u32[]{:S(2)}, u32[]{:S(2)}) collective-permute-start(bf16[128,256]{1,0:T(8,128)(2,1)S(1)} %copy-done.14), channel_id=1, source_target_pairs={{0,8},{8,0},{1,9},{9,1},{2,10},{10,2},{3,11},{11,3},{4,12},{12,4},... | collective-permute-start | bytes 196616 | tf_op jit(solution)/shard_map/ppermute | solution.py:255
  23.5 2.7 %collective-permute-done = bf16[128,256]{1,0:T(8,128)(2,1)S(1)} collective-permute-done((bf16[128,256]{1,0:T(8,128)(2,1)S(1)}, bf16[128,256]{1,0:T(8,128)(2,1)S(1)}, u32[]{:S(2)}, u32[]{:S(2)}) %collective-permute-start) | collective-permute-done | bytes 65568 | tf_op jit(solution)/shard_map/ppermute | solution.py:255
  26.3 3.3 %collective-permute-start.2 = (bf16[1296,256]{1,0:T(8,128)(2,1)S(1)}, bf16[1296,256]{1,0:T(8,128)(2,1)S(1)}, u32[]{:S(2)}, u32[]{:S(2)}) collective-permute-start(bf16[1296,256]{1,0:T(8,128)(2,1)S(1)} %fusion.1.refs_0_), channel_id=1, source_target_pairs={{0,2},{2,4},{4,6},{6,0},{1,3},{3,5},{5,7},{7,1},{8,10},{10,12},{12... | collective-permute-start | bytes 1990664 | tf_op jit(solution)/shard_map/ppermute | solution.py:268
  29.6 4.4 %collective-permute-start.4 = (bf16[1296,256]{1,0:T(8,128)(2,1)S(1)}, bf16[1296,256]{1,0:T(8,128)(2,1)S(1)}, u32[]{:S(2)}, u32[]{:S(2)}) collective-permute-start(bf16[1296,256]{1,0:T(8,128)(2,1)S(1)} %fusion.1.refs_0_), channel_id=1, source_target_pairs={{0,4},{2,6},{4,0},{6,2},{1,5},{3,7},{5,1},{7,3},{8,12},{10,14},{12... | collective-permute-start | bytes 1990664 | tf_op jit(solution)/shard_map/ppermute | solution.py:268
  33.9 3.1 %collective-permute-start.6 = (bf16[1296,256]{1,0:T(8,128)(2,1)S(1)}, bf16[1296,256]{1,0:T(8,128)(2,1)S(1)}, u32[]{:S(2)}, u32[]{:S(2)}) collective-permute-start(bf16[1296,256]{1,0:T(8,128)(2,1)S(1)} %fusion.1.refs_0_), channel_id=1, source_target_pairs={{0,6},{2,0},{4,2},{6,4},{1,7},{3,1},{5,3},{7,5},{8,14},{10,8},{12,... | collective-permute-start | bytes 1990664 | tf_op jit(solution)/shard_map/ppermute | solution.py:268
  37.0 3.7 %all-to-all-start = ((bf16[8,40,128]{2,1,0:T(8,128)(2,1)}), bf16[8,40,128]{2,1,0:T(8,128)(2,1)S(1)}, u32[]{:S(2)}, u32[]{:S(2)}) async-start(bf16[8,40,128]{2,1,0:T(8,128)(2,1)} %get-tuple-element.18), calls=%async_computation | async-start | bytes 163840 | tf_op jit(solution)/shard_map/all_to_all | solution.py:170
  40.7 5.8 %all-to-all-done.arrived_ref = bf16[8,40,128]{2,1,0:T(8,128)(2,1)S(1)} async-done(((bf16[8,40,128]{2,1,0:T(8,128)(2,1)}), bf16[8,40,128]{2,1,0:T(8,128)(2,1)S(1)}, u32[]{:S(2)}, u32[]{:S(2)}) %all-to-all-start) | async-done | bytes 81952 | tf_op jit(solution)/shard_map/all_to_all | solution.py:170
  47.2 14.3 %all-to-all-start.1 = ((bf16[8,24,128]{2,1,0:T(8,128)(2,1)}), bf16[8,24,128]{2,1,0:T(8,128)(2,1)S(1)}, u32[]{:S(2)}, u32[]{:S(2)}) async-start(bf16[8,24,128]{2,1,0:T(8,128)(2,1)} %plane.1), calls=%async_computation.1 | async-start | bytes 98304 | tf_op jit(solution)/shard_map/all_to_all | solution.py:180
  61.5 7.3 %collective-permute-start.1 = (bf16[1296,256]{1,0:T(8,128)(2,1)S(1)}, bf16[1296,256]{1,0:T(8,128)(2,1)}, u32[]{:S(2)}, u32[]{:S(2)}) collective-permute-start(bf16[1296,256]{1,0:T(8,128)(2,1)S(1)} %fusion.1.refs_0_), channel_id=1, source_target_pairs={{0,1},{1,0},{2,3},{3,2},{4,5},{5,4},{6,7},{7,6},{8,9},{9,8},{10,11... | collective-permute-start | bytes 1990664 | tf_op jit(solution)/shard_map/ppermute | solution.py:540
  68.8 1.9 %collective-permute-start.3 = (bf16[1296,256]{1,0:T(8,128)(2,1)S(1)}, bf16[1296,256]{1,0:T(8,128)(2,1)}, u32[]{:S(2)}, u32[]{:S(2)}) collective-permute-start(bf16[1296,256]{1,0:T(8,128)(2,1)S(1)} %collective-permute-done.2.refs_2_), channel_id=1, source_target_pairs={{0,1},{1,0},{2,3},{3,2},{4,5},{5,4},{6,7},{7,6},{8,9},{9,8},{10,11... | collective-permute-start | bytes 1990664 | tf_op jit(solution)/shard_map/ppermute | solution.py:540
  70.7 2.4 %collective-permute-start.5 = (bf16[1296,256]{1,0:T(8,128)(2,1)S(1)}, bf16[1296,256]{1,0:T(8,128)(2,1)}, u32[]{:S(2)}, u32[]{:S(2)}) collective-permute-start(bf16[1296,256]{1,0:T(8,128)(2,1)S(1)} %collective-permute-done.4.refs_4_), channel_id=1, source_target_pairs={{0,1},{1,0},{2,3},{3,2},{4,5},{5,4},{6,7},{7,6},{8,9},{9,8},{10,11... | collective-permute-start | bytes 1990664 | tf_op jit(solution)/shard_map/ppermute | solution.py:540
  73.2 1.9 %collective-permute-start.7 = (bf16[1296,256]{1,0:T(8,128)(2,1)S(1)}, bf16[1296,256]{1,0:T(8,128)(2,1)}, u32[]{:S(2)}, u32[]{:S(2)}) collective-permute-start(bf16[1296,256]{1,0:T(8,128)(2,1)S(1)} %collective-permute-done.6.refs_6_), channel_id=1, source_target_pairs={{0,1},{1,0},{2,3},{3,2},{4,5},{5,4},{6,7},{7,6},{8,9},{9,8},{10,11... | collective-permute-start | bytes 1990664 | tf_op jit(solution)/shard_map/ppermute | solution.py:540
  75.2 8.0 %all_to_all.36.back_ref = bf16[8,32,128]{2,1,0:T(8,128)(2,1)S(1)} all-to-all(bf16[8,32,128]{2,1,0:T(8,128)(2,1)S(1)} %before.1), channel_id=1, replica_groups=mesh['zb'=8,'zr'=2,'ya'=2,'yb'=2,'x'=4,'c'=2] {'zr','ya','yb'}, dimensions={0} | all-to-all | bytes 131072 | tf_op jit(solution)/shard_map/all_to_all | solution.py:189
  84.3 3.4 %all-to-all-start.3 = ((bf16[8,128,128]{2,1,0:T(8,128)(2,1)}), bf16[8,128,128]{2,1,0:T(8,128)(2,1)S(1)}, u32[]{:S(2)}, u32[]{:S(2)}) async-start(bf16[8,128,128]{2,1,0:T(8,128)(2,1)} %gated.1), calls=%async_computation.3 | async-start | bytes 524288 | tf_op jit(solution)/shard_map/all_to_all | solution.py:536
  87.9 5.9 %all-to-all-done.3 = bf16[8,128,128]{2,1,0:T(8,128)(2,1)S(1)} async-done(((bf16[8,128,128]{2,1,0:T(8,128)(2,1)}), bf16[8,128,128]{2,1,0:T(8,128)(2,1)S(1)}, u32[]{:S(2)}, u32[]{:S(2)}) %all-to-all-start.3) | async-done | bytes 262176 | tf_op jit(solution)/shard_map/all_to_all | solution.py:536
  93.8 9.4 %all-gather = bf16[16,128,128]{2,1,0:T(8,128)(2,1)S(1)} all-gather(bf16[8,128,128]{2,1,0:T(8,128)(2,1)S(1)} %all-to-all-done.3), channel_id=2, replica_groups=mesh['zb'=8,'zr'=2,'ya'=2,'yb'=2,'x'=4,'c'=2] {'c'}, dimensions={0}, use_global_device_ids=true | all-gather | bytes 786432 | tf_op jit(solution)/shard_map/all_gather | solution.py:537
  104.3 3.7 %middle.1 = (bf16[8,256,256]{2,1,0:T(8,128)(2,1)S(1)}, bf16[128,256]{1,0:T(8,128)(2,1)S(1)}) custom-call(s32[9]{0:T(128)S(1)} %stack.83.place_ref, bf16[2,8,128,128]{3,2,1,0:T(8,128)(2,1)S(1)} %bitcast.29, bf16[1296,256]{1,0:T(8,128)(2,1)S(1)} %fusion.1.refs_0_, bf16[1296,256]{1,0:T(8,128)(2,1)} %collective-permute-done.1.refs_1_, ...), custom_call_target="tpu_custom_call" | custom-call | tf_op jit(solution)/shard_map/middle/pallas_call | solution.py:316
  108.0 4.0 %feed_enter.1 = (bf16[2,4,128,256]{3,2,1,0:T(8,128)(2,1)S(1)}, bf16[256,352]{1,0:T(8,128)(2,1)S(1)}) custom-call(s32[1]{0:T(128)} %bitcast.core_ref, bf16[8,256,256]{2,1,0:T(8,128)(2,1)S(1)} %get-tuple-element.23.rows_ref, bf16[16,3,352,128]{3,2,1,0:T(8,128)(2,1)} %bitcast.36), custom_call_target="tpu_custom_call" | custom-call | flops 922746880 | bytes 3604480 | tf_op jit(solution)/shard_map/feed_enter/pallas_call | solution.py:415
  112.0 2.3 %collective-permute-start.8 = (bf16[2,4,128,256]{3,2,1,0:T(8,128)(2,1)S(1)}, bf16[2,4,128,256]{3,2,1,0:T(8,128)(2,1)S(1)}, u32[]{:S(2)}, u32[]{:S(2)}) collective-permute-start(bf16[2,4,128,256]{3,2,1,0:T(8,128)(2,1)S(1)} %get-tuple-element.25), channel_id=1, source_target_pairs={{0,1},{1,0},{2,3},{3,2},{4,5},{5,4},{6,7},{7,6},{8,9},{9,8},{10,11... | collective-permute-start | bytes 1572872 | tf_op jit(solution)/shard_map/ppermute | solution.py:544
  114.3 2.1 %feed_leave.1.mine_ref = f32[2,4,128,256]{3,2,1,0:T(8,128)S(1)} custom-call(s32[1]{0:T(128)} %bitcast.core_ref, bf16[256,352]{1,0:T(8,128)(2,1)S(1)} %get-tuple-element.24.hidden_ref, bf16[16,3,352,128]{3,2,1,0:T(8,128)(2,1)} %bitcast.37), custom_call_target="tpu_custom_call" | custom-call | flops 184549376 | bytes 720896 | tf_op jit(solution)/shard_map/feed_leave/pallas_call | solution.py:439
  116.6 12.6 %all_to_all.37.arrived_ref = bf16[8,128,256]{2,1,0:T(8,128)(2,1)S(1)} all-to-all(bf16[8,128,256]{2,1,0:T(8,128)(2,1)S(1)} %join.1), channel_id=1, replica_groups=mesh['zb'=8,'zr'=2,'ya'=2,'yb'=2,'x'=4,'c'=2] {'yb','x'}, dimensions={0} | all-to-all | bytes 1048576 | tf_op jit(solution)/shard_map/all_to_all | solution.py:546
  129.4 7.8 %all_to_all.38.moments_ref = f32[8,1,256]{2,1,0:T(1,128)S(1)} all-to-all(f32[8,1,256]{2,1,0:T(1,128)S(1)} %get-tuple-element.27), channel_id=1, replica_groups=mesh['zb'=8,'zr'=2,'ya'=2,'yb'=2,'x'=4,'c'=2] {'x','c'}, dimensions={0} | all-to-all | bytes 16384 | tf_op jit(solution)/shard_map/all_to_all | solution.py:556
  (68 shorter events, 6.4 us)
Async XLA Ops:
  6.5 12.7 %copy-start.5 = (bf16[128,128]{1,0:T(8,128)(2,1)S(1)}, bf16[128,128]{1,0:T(8,128)(2,1)}, u32[]{:S(2)}) copy-start(bf16[128,128]{1,0:T(8,128)(2,1)} %onward_ref.1) | copy-start | bytes 98308
  6.6 12.7 %copy-start.6 = (bf16[128,128]{1,0:T(8,128)(2,1)S(1)}, bf16[128,128]{1,0:T(8,128)(2,1)}, u32[]{:S(2)}) copy-start(bf16[128,128]{1,0:T(8,128)(2,1)} %reverse_ref.1) | copy-start | bytes 98308
  6.6 14.6 %copy-start.14 = (bf16[128,256]{1,0:T(8,128)(2,1)S(1)}, bf16[128,256]{1,0:T(8,128)(2,1)}, u32[]{:S(2)}) copy-start(bf16[128,256]{1,0:T(8,128)(2,1)} %param.27) | copy-start | bytes 196612
  6.6 16.8 %copy-start.15 = (f32[256]{0:T(256)S(1)}, f32[256]{0:T(256)}, u32[]{:S(2)}) copy-start(f32[256]{0:T(256)} %param.29) | copy-start | bytes 3076
  6.6 16.8 %copy-start.16 = (f32[256]{0:T(256)S(1)}, f32[256]{0:T(256)}, u32[]{:S(2)}) copy-start(f32[256]{0:T(256)} %param.30) | copy-start | bytes 3076
  6.6 101.4 %all-gather.3.cloned.1.call-start = ((), (), s32[]{:S(2)}) async-start(), calls=%async_computation.7 | async-start | bytes 4595712 | tf_op jit(solution)/shard_map/all_gather | solution.py:238
  7.6 18.6 %copy-start.13 = (bf16[1024,256]{1,0:T(8,128)(2,1)S(1)}, bf16[1024,256]{1,0:T(8,128)(2,1)}, u32[]{:S(2)}) copy-start(bf16[1024,256]{1,0:T(8,128)(2,1)} %param.28) | copy-start | bytes 1572868
  19.1 64.0 %copy-start.2 = (bf16[128,128]{1,0:T(8,128)(2,1)S(1)}, bf16[128,128]{1,0:T(8,128)(2,1)}, u32[]{:S(2)}) copy-start(bf16[128,128]{1,0:T(8,128)(2,1)} %gate_ref.1) | copy-start | bytes 98308
  19.1 64.0 %copy-start.12 = (f32[128]{0:T(128)S(1)}, f32[128]{0:T(128)}, u32[]{:S(2)}) copy-start(f32[128]{0:T(128)} %param.26) | copy-start | bytes 1540
  21.2 5.0 %collective-permute-start = (bf16[128,256]{1,0:T(8,128)(2,1)S(1)}, bf16[128,256]{1,0:T(8,128)(2,1)S(1)}, u32[]{:S(2)}, u32[]{:S(2)}) collective-permute-start(bf16[128,256]{1,0:T(8,128)(2,1)S(1)} %copy-done.14), channel_id=1, source_target_pairs={{0,8},{8,0},{1,9},{9,1},{2,10},{10,2},{3,11},{11,3},{4,12},{12,4},... | collective-permute-start | bytes 196616 | tf_op jit(solution)/shard_map/ppermute | solution.py:255
  26.3 42.5 %collective-permute-start.2 = (bf16[1296,256]{1,0:T(8,128)(2,1)S(1)}, bf16[1296,256]{1,0:T(8,128)(2,1)S(1)}, u32[]{:S(2)}, u32[]{:S(2)}) collective-permute-start(bf16[1296,256]{1,0:T(8,128)(2,1)S(1)} %fusion.1.refs_0_), channel_id=1, source_target_pairs={{0,2},{2,4},{4,6},{6,0},{1,3},{3,5},{5,7},{7,1},{8,10},{10,12},{12... | collective-permute-start | bytes 1990664 | tf_op jit(solution)/shard_map/ppermute | solution.py:268
  29.6 41.2 %collective-permute-start.4 = (bf16[1296,256]{1,0:T(8,128)(2,1)S(1)}, bf16[1296,256]{1,0:T(8,128)(2,1)S(1)}, u32[]{:S(2)}, u32[]{:S(2)}) collective-permute-start(bf16[1296,256]{1,0:T(8,128)(2,1)S(1)} %fusion.1.refs_0_), channel_id=1, source_target_pairs={{0,4},{2,6},{4,0},{6,2},{1,5},{3,7},{5,1},{7,3},{8,12},{10,14},{12... | collective-permute-start | bytes 1990664 | tf_op jit(solution)/shard_map/ppermute | solution.py:268
  33.9 39.2 %collective-permute-start.6 = (bf16[1296,256]{1,0:T(8,128)(2,1)S(1)}, bf16[1296,256]{1,0:T(8,128)(2,1)S(1)}, u32[]{:S(2)}, u32[]{:S(2)}) collective-permute-start(bf16[1296,256]{1,0:T(8,128)(2,1)S(1)} %fusion.1.refs_0_), channel_id=1, source_target_pairs={{0,6},{2,0},{4,2},{6,4},{1,7},{3,1},{5,3},{7,5},{8,14},{10,8},{12,... | collective-permute-start | bytes 1990664 | tf_op jit(solution)/shard_map/ppermute | solution.py:268
  37.0 9.5 %all-to-all-start = ((bf16[8,40,128]{2,1,0:T(8,128)(2,1)}), bf16[8,40,128]{2,1,0:T(8,128)(2,1)S(1)}, u32[]{:S(2)}, u32[]{:S(2)}) async-start(bf16[8,40,128]{2,1,0:T(8,128)(2,1)} %get-tuple-element.18), calls=%async_computation | async-start | bytes 163840 | tf_op jit(solution)/shard_map/all_to_all | solution.py:170
  47.2 27.9 %all-to-all-start.1 = ((bf16[8,24,128]{2,1,0:T(8,128)(2,1)}), bf16[8,24,128]{2,1,0:T(8,128)(2,1)S(1)}, u32[]{:S(2)}, u32[]{:S(2)}) async-start(bf16[8,24,128]{2,1,0:T(8,128)(2,1)} %plane.1), calls=%async_computation.1 | async-start | bytes 98304 | tf_op jit(solution)/shard_map/all_to_all | solution.py:180
  61.5 41.7 %collective-permute-start.1 = (bf16[1296,256]{1,0:T(8,128)(2,1)S(1)}, bf16[1296,256]{1,0:T(8,128)(2,1)}, u32[]{:S(2)}, u32[]{:S(2)}) collective-permute-start(bf16[1296,256]{1,0:T(8,128)(2,1)S(1)} %fusion.1.refs_0_), channel_id=1, source_target_pairs={{0,1},{1,0},{2,3},{3,2},{4,5},{5,4},{6,7},{7,6},{8,9},{9,8},{10,11... | collective-permute-start | bytes 1990664 | tf_op jit(solution)/shard_map/ppermute | solution.py:540
  68.8 34.4 %collective-permute-start.3 = (bf16[1296,256]{1,0:T(8,128)(2,1)S(1)}, bf16[1296,256]{1,0:T(8,128)(2,1)}, u32[]{:S(2)}, u32[]{:S(2)}) collective-permute-start(bf16[1296,256]{1,0:T(8,128)(2,1)S(1)} %collective-permute-done.2.refs_2_), channel_id=1, source_target_pairs={{0,1},{1,0},{2,3},{3,2},{4,5},{5,4},{6,7},{7,6},{8,9},{9,8},{10,11... | collective-permute-start | bytes 1990664 | tf_op jit(solution)/shard_map/ppermute | solution.py:540
  70.7 32.5 %collective-permute-start.5 = (bf16[1296,256]{1,0:T(8,128)(2,1)S(1)}, bf16[1296,256]{1,0:T(8,128)(2,1)}, u32[]{:S(2)}, u32[]{:S(2)}) collective-permute-start(bf16[1296,256]{1,0:T(8,128)(2,1)S(1)} %collective-permute-done.4.refs_4_), channel_id=1, source_target_pairs={{0,1},{1,0},{2,3},{3,2},{4,5},{5,4},{6,7},{7,6},{8,9},{9,8},{10,11... | collective-permute-start | bytes 1990664 | tf_op jit(solution)/shard_map/ppermute | solution.py:540
  73.2 30.1 %copy-start = (bf16[1296,256]{1,0:T(8,128)(2,1)}, bf16[1296,256]{1,0:T(8,128)(2,1)S(1)}, u32[]{:S(2)}) copy-start(bf16[1296,256]{1,0:T(8,128)(2,1)S(1)} %collective-permute-done.6.refs_6_) | copy-start | bytes 1990660
  73.2 30.0 %collective-permute-start.7 = (bf16[1296,256]{1,0:T(8,128)(2,1)S(1)}, bf16[1296,256]{1,0:T(8,128)(2,1)}, u32[]{:S(2)}, u32[]{:S(2)}) collective-permute-start(bf16[1296,256]{1,0:T(8,128)(2,1)S(1)} %collective-permute-done.6.refs_6_), channel_id=1, source_target_pairs={{0,1},{1,0},{2,3},{3,2},{4,5},{5,4},{6,7},{7,6},{8,9},{9,8},{10,11... | collective-permute-start | bytes 1990664 | tf_op jit(solution)/shard_map/ppermute | solution.py:540
  84.3 9.5 %all-to-all-start.3 = ((bf16[8,128,128]{2,1,0:T(8,128)(2,1)}), bf16[8,128,128]{2,1,0:T(8,128)(2,1)S(1)}, u32[]{:S(2)}, u32[]{:S(2)}) async-start(bf16[8,128,128]{2,1,0:T(8,128)(2,1)} %gated.1), calls=%async_computation.3 | async-start | bytes 524288 | tf_op jit(solution)/shard_map/all_to_all | solution.py:536
  112.0 4.4 %collective-permute-start.8 = (bf16[2,4,128,256]{3,2,1,0:T(8,128)(2,1)S(1)}, bf16[2,4,128,256]{3,2,1,0:T(8,128)(2,1)S(1)}, u32[]{:S(2)}, u32[]{:S(2)}) collective-permute-start(bf16[2,4,128,256]{3,2,1,0:T(8,128)(2,1)S(1)} %get-tuple-element.25), channel_id=1, source_target_pairs={{0,1},{1,0},{2,3},{3,2},{4,5},{5,4},{6,7},{7,6},{8,9},{9,8},{10,11... | collective-permute-start | bytes 1572872 | tf_op jit(solution)/shard_map/ppermute | solution.py:544
  116.6 20.6 %copy-start.7 = (f32[256]{0:T(256)S(1)}, f32[256]{0:T(256)}, u32[]{:S(2)}) copy-start(f32[256]{0:T(256)} %param.34) | copy-start | bytes 3076
  116.6 20.6 %copy-start.8 = (f32[256]{0:T(256)S(1)}, f32[256]{0:T(256)}, u32[]{:S(2)}) copy-start(f32[256]{0:T(256)} %param.35) | copy-start | bytes 3076
  (6 other events, 64.3 us)
Sparse Core Ops, SparseCore 0:
  19.3 75.1 all-gather.2
